TPU v7x, 512 devices: a 4x2x32 block of a 4x8x32 slice. The times are simulated.
512 devices in a mesh: grp: 2 (over y), sp: 32 (over z), tp: 8 (over x, core).
Axes of the slice: x: 4, y: 2, z: 32, core: 2. Of those that a mesh axis runs over, the one named last changes fastest.
The devices are a block of a 4x8x32 slice.
Arguments:
- queries: bfloat16 [32768, 1024], P(('grp', 'sp'), 'tp'), parts along dimension 0, may hold values from -6 to 6
- memory_keys: bfloat16 [32768, 1024], P(('grp', 'sp'), 'tp'), parts along dimension 0, may hold values from -6 to 6
- memory_values: bfloat16 [32768, 1024], P(('grp', 'sp'), 'tp'), parts along dimension 0, may hold values from -6 to 6
- output_preactivation: bfloat16 [32768, 1024], P(('grp', 'sp'), 'tp'), parts along dimension 0, may hold values from -12 to 12
- input_preactivation: float32 [8, 32768], P('tp', ('grp', 'sp')), parts along dimension 1, may hold values from -6 to 140
- forget_preactivation: float32 [8, 32768], P('tp', ('grp', 'sp')), parts along dimension 1, as said below
- extra_forget_terms: float32 [8, 32768], P('tp', ('grp', 'sp')), parts along dimension 1, may hold values from -1 to 0, as said below
- head_norm_gain: float32 [128], replicated, may hold values from 0.1 to 1.9
- output_projection_matrix: bfloat16 [1024, 2048], P('tp'), may hold values from -0.1875 to 0.1875
- residual: bfloat16 [32768, 2048], P(('grp', 'sp', 'tp')), parts along dimension 0, may hold values from -6 to 6
- feedforward_norm_gain: float32 [2048], replicated, may hold values from 0.1 to 1.9
- feedforward_up_matrix: bfloat16 [2048, 8192], P('sp', 'tp'), may hold values from -0.125 to 0.125
- feedforward_down_matrix: bfloat16 [8192, 2048], P('tp', 'sp'), may hold values from -0.0625 to 0.0625
Outputs:
- layer_out: bfloat16 [32768, 2048], P(('grp', 'sp', 'tp')), parts along dimension 0
There are 2 independent parts, one for each index of `grp`. A program takes and returns all parts, laid end to end along the dimension named above; an argument that names none is the same for every part. Nothing has to cross between parts.
Inputs may be any that keep to these rules, and one draw needn't show every extreme that they name: `forget_preactivation`: forget gate pre-activations. `extra_forget_terms`: extra log forget terms, zero at most positions.
All inputs are finite; a program needn't handle non-finite values.
Results may differ from a plain program's by a relative error of at most 0.018.
Values may be sent and summed in bfloat16 or wider, within the bound.
No kernel may reach another device: no remote copies, remote signals or barrier semaphores. Data moves between devices by JAX's collectives and lax.ppermute only.
A program may use at most 64 MiB of HBM per device.

v0:
```python
import jax
import jax.numpy as jnp
from jax import lax
from jax.sharding import PartitionSpec as P

BLOCK = 128


neg_big = -1e30
norm_eps = 1e-06
highest = lax.Precision.HIGHEST


def turned_gather(arrays, axis, dims):
    turned = [jnp.moveaxis(a, dim, 0) for a, dim in zip(arrays, dims)]
    both = jnp.concatenate([t.reshape(len(t), -1) for t in turned], axis=1)
    filled, at, outs = (lax.all_gather(both, axis, axis=0, tiled=True), 0, [])
    for t, dim in zip(turned, dims):
        piece = filled[:, at : at + t[0].size].reshape(-1, *t.shape[1:])
        outs.append(jnp.moveaxis(piece, 0, dim))
        at += t[0].size
    return tuple(outs)


def all_in_one(x, axis):
    leaves = jax.tree.leaves(x)
    order = sorted(range(len(leaves)), key=lambda k: -leaves[k].size)
    width = (1, *leaves[order[0]].shape)[-1]
    lines = [
        jnp.pad(leaves[k].reshape(-1), (0, -leaves[k].size % width)).reshape(-1, width)
        for k in order
    ]
    both, at, found = (lax.all_gather(jnp.concatenate(lines), axis), 0, {})
    for k, line in zip(order, lines):
        piece = both[:, at : at + len(line)].reshape(len(both), -1)
        found[k] = piece[:, : leaves[k].size].reshape(-1, *leaves[k].shape)
        at += len(line)
    numbers = iter(range(len(leaves)))
    return jax.tree.map(lambda _: found[next(numbers)], x)


def prefix_2(part, axis, combine, identity):
    place = lax.axis_index(axis)
    gathered = all_in_one(part, axis)
    state = jax.tree.map(lambda a, e: jnp.zeros_like(a) + jnp.asarray(e, a.dtype), part, identity)

    def one(step, state):
        return combine(
            state, jax.tree.map(lambda a: lax.dynamic_index_in_dim(a, step, 0, False), gathered)
        )

    return lax.fori_loop(0, place, one, state)


def cut_along(x, dim, length):
    before, after = (x.shape[:dim], x.shape[dim + 1 :])
    return jnp.moveaxis(x.reshape(*before, length, -1, *after), dim, 0)


def sum_at_owner(x, axis, dim):
    length = lax.axis_size(axis)
    blocks = lax.all_to_all(cut_along(x, dim, length), axis, 0, 0, tiled=True)
    return jnp.sum(blocks.astype(jnp.float32), axis=0)


def laid_out(blocks, dim):
    blocks = jnp.moveaxis(blocks, 0, dim)
    lengths = blocks.shape
    return blocks.reshape(*lengths[:dim], lengths[dim] * lengths[dim + 1], *lengths[dim + 2 :])


def copy_for_each(x, axis):
    copies = jnp.broadcast_to(x, (lax.axis_size(axis), *x.shape))
    return lax.all_to_all(copies, axis, split_axis=0, concat_axis=0, tiled=True)


def gather_directly(x, axis, dim):
    return laid_out(copy_for_each(x, axis), dim)


def rms_norm(tensor, gain_vec):
    mean_sq = jnp.mean(tensor * tensor, axis=-1, keepdims=True)
    return tensor * lax.rsqrt(mean_sq + norm_eps) * gain_vec


def combine(earlier, later):
    total_e, max_e, memory_e = earlier
    total_l, max_l, memory_l = later
    carried = total_l + max_e
    new_max = jnp.maximum(carried, max_l)
    old_part = jnp.exp(carried - new_max)
    new_part = jnp.exp(max_l - new_max)
    return (
        total_e + total_l,
        new_max,
        old_part[..., None, None] * memory_e + new_part[..., None, None] * memory_l,
    )


def block_summary(key_blk, val_blk, gate_blk, decay_logarithm):
    block_total = decay_logarithm[..., -1]
    tail_log = block_total[..., None] - decay_logarithm + gate_blk
    tail_max = jnp.max(tail_log, axis=-1)
    weights = jnp.exp(tail_log - tail_max[..., None])
    memory = jnp.einsum("bhsv,bhsk->bhvk", weights[..., None] * val_blk, key_blk, precision=highest)
    return (block_total, tail_max, memory)


def shards(
    queries,
    memory_keys,
    memory_values,
    output_preactivation,
    input_preactivation,
    forget_preactivation,
    extra_forget_terms,
    head_norm_gain,
    output_projection_matrix,
    residual,
    feedforward_norm_gain,
    feedforward_up_matrix,
    feedforward_down_matrix,
):
    tok_count = queries.shape[0]
    head_count = input_preactivation.shape[0]
    head_dim = queries.shape[1] // head_count
    block_len = BLOCK
    block_count = tok_count // block_len
    whole_up, whole_down = turned_gather(
        (feedforward_up_matrix, feedforward_down_matrix), "sp", (0, 1)
    )

    def to_blocks(tensor):
        return (
            tensor.astype(jnp.float32)
            .reshape(block_count, block_len, head_count, head_dim)
            .transpose(0, 2, 1, 3)
        )

    def gate_block_list(tensor):
        return tensor.reshape(head_count, block_count, block_len).transpose(1, 0, 2)

    query_blk = to_blocks(queries)
    key_blk = to_blocks(memory_keys) * head_dim ** (-0.5)
    val_blk = to_blocks(memory_values)
    gate_blk = gate_block_list(input_preactivation)
    decay_logarithm = jnp.cumsum(
        gate_block_list(jax.nn.log_sigmoid(forget_preactivation) + extra_forget_terms), axis=-1
    )
    summaries = block_summary(key_blk, val_blk, gate_blk, decay_logarithm)
    zero_heads = jnp.zeros((head_count,), jnp.float32)
    zero_memory = jnp.zeros((head_count, head_dim, head_dim), jnp.float32)
    zero_state = (zero_heads, jnp.full((head_count,), neg_big, jnp.float32), zero_memory)
    prefixes = []
    running = zero_state
    for block_idx in range(block_count):
        prefixes.append(running)
        running = combine(running, tuple((member[block_idx] for member in summaries)))
    before = prefix_2(running, "sp", combine, zero_state)
    anchor = (zero_heads, zero_heads, zero_memory)
    incoming = combine(anchor, before)
    starts = [combine(incoming, prefix) for prefix in prefixes]
    start_max = jnp.stack([each_state[1] for each_state in starts])
    start_memory = jnp.stack([each_state[2] for each_state in starts])
    causal = lax.broadcasted_iota(jnp.int32, (block_len, block_len), 0) >= lax.broadcasted_iota(
        jnp.int32, (block_len, block_len), 1
    )
    log_weight = (
        decay_logarithm[..., :, None] - decay_logarithm[..., None, :] + gate_blk[..., None, :]
    )
    log_weight = jnp.where(causal, log_weight, neg_big)
    carry_log = decay_logarithm + start_max[..., None]
    row_max = jnp.maximum(jnp.max(log_weight, axis=-1), carry_log)
    scores = jnp.einsum("bhtd,bhsd->bhts", query_blk, key_blk, precision=highest) * jnp.exp(
        log_weight - row_max[..., None]
    )
    carry_scale = jnp.exp(carry_log - row_max)
    hidden = jnp.einsum("bhts,bhsv->bhtv", scores, val_blk, precision=highest)
    hidden = hidden + carry_scale[..., None] * jnp.einsum(
        "bhvk,bhtk->bhtv", start_memory, query_blk, precision=highest
    )
    hidden = hidden.transpose(0, 2, 1, 3).reshape(tok_count, head_count, head_dim)
    gated = rms_norm(hidden, head_norm_gain) * jax.nn.sigmoid(
        output_preactivation.astype(jnp.float32).reshape(tok_count, head_count, head_dim)
    )
    mixed = gated.reshape(tok_count, head_count * head_dim).astype(jnp.bfloat16)
    branch = sum_at_owner(
        jnp.dot(mixed, output_projection_matrix, preferred_element_type=jnp.float32).astype(
            jnp.bfloat16
        ),
        "tp",
        0,
    )
    mid_state = (residual.astype(jnp.float32) + branch).astype(jnp.bfloat16)
    normed = rms_norm(mid_state.astype(jnp.float32), feedforward_norm_gain).astype(jnp.bfloat16)
    normed_all = gather_directly(normed, "tp", 0)
    upward = jnp.dot(normed_all, whole_up, preferred_element_type=jnp.float32)
    active = jnp.square(jax.nn.relu(upward)).astype(jnp.bfloat16)
    mlp_sum = sum_at_owner(
        jnp.dot(active, whole_down, preferred_element_type=jnp.float32).astype(jnp.bfloat16),
        "tp",
        0,
    )
    return (mid_state.astype(jnp.float32) + mlp_sum).astype(jnp.bfloat16)


def solution(mesh):
    in_specs = (
        P(("grp", "sp"), "tp"),
        P(("grp", "sp"), "tp"),
        P(("grp", "sp"), "tp"),
        P(("grp", "sp"), "tp"),
        P("tp", ("grp", "sp")),
        P("tp", ("grp", "sp")),
        P("tp", ("grp", "sp")),
        P(),
        P("tp", None),
        P(("grp", "sp", "tp"), None),
        P(),
        P("sp", "tp"),
        P("tp", "sp"),
    )
    out_specs = P(("grp", "sp", "tp"), None)
    return jax.shard_map(shards, mesh=mesh, in_specs=in_specs, out_specs=out_specs, check_vma=False)
```

profile of v0, /device:TPU:33, one launch (start us, length us, event | category | flops | bytes accessed | tf_op | source)
XLA Modules:
  0.0 381.0 jit_solution(692592151489835851)
XLA Ops:
  6.5 0.0 copy-start
  6.6 0.0 copy-start.6
  6.6 0.0 all-gather.7.cloned.1.call-start
  6.6 0.8 fusion.40
  7.3 1.2 reduce_window_sum.11
  8.6 0.2 slice_reduce_fusion
  8.8 0.7 fusion.45
  9.4 0.9 fusion.39
  10.3 0.6 fusion.46
  19.9 0.9 convert_multiply_fusion.2
  22.1 0.8 subtract_exponential_fusion.1
  22.8 1.6 fusion.28
  24.5 0.6 maximum_bitcast_fusion.2
  25.1 0.1 all-gather.7.cloned.1.call-update
  25.2 0.1 all-gather.5.cloned.1.call-start
  25.2 1.7 pad_maximum_fusion
  26.9 0.1 all-gather.5.cloned.1.call-update
  27.0 0.0 copy-start.4
  27.0 0.1 copy.32
  27.2 0.0 copy-done.6
  27.2 0.2 select_reduce_fusion
  27.4 139.0 %all-gather.7.cloned.1.call-done = f32[32,130,128]{2,1,0:T(8,128)} async-done(((f32[1,130,128]{2,1,0:T(8,128)}), f32[32,130,128]{2,1,0:T(8,128)}) %all-gather.7.cloned.1.call-update) | async-done | bytes 2129936 | tf_op jit(solution)/shard_map/all_gather | solution.py:33
  166.4 0.0 copy-done.4
  166.4 1.7 fusion.44
  168.2 0.0 copy-start.2
  168.2 1.8 slice_bitcast_fusion
  169.9 0.0 copy-start.1
  170.0 0.0 copy-start.8
  170.0 0.0 copy-start.5
  171.1 0.1 maximum_bitcast_fusion.3
  171.2 0.1 subtract_exponential_fusion
  171.3 0.0 copy-done.2
  171.3 1.1 fusion.13
  172.4 0.0 copy-done.1
  172.5 0.4 fusion.47
  172.8 0.5 multiply_reduce_fusion
  173.4 0.0 copy-done.8
  173.4 0.0 copy-done.5
  173.4 0.1 fusion.27
  173.5 0.0 copy-done
  173.5 0.7 convolution_convert_fusion
  174.2 52.1 %all_to_all.15 = bf16[8,64,2048]{2,1,0:T(8,128)(2,1)S(1)} all-to-all(bf16[8,64,2048]{2,1,0:T(8,128)(2,1)S(1)} %bitcast.121), channel_id=1, replica_groups=mesh['grp'=2,'sp'=32,'tp'=8] {'tp'}, dimensions={0} | all-to-all | bytes 4194304 | tf_op jit(solution)/shard_map/all_to_all | solution.py:62
  226.3 0.0 copy-start.3
  226.4 0.0 copy-start.7
  226.4 0.4 convert_reduce_fusion.1
  226.7 0.6 copy-done.3
  227.3 0.2 fusion.15
  227.5 0.0 copy-done.7
  227.5 0.1 fusion.17
  227.6 0.2 broadcast_in_dim.21
  227.9 29.7 %all_to_all.16 = bf16[8,64,2048]{2,1,0:T(8,128)(2,1)S(1)} all-to-all(bf16[8,64,2048]{2,1,0:T(8,128)(2,1)S(1)} %broadcast_in_dim.21), channel_id=1, replica_groups=mesh['grp'=2,'sp'=32,'tp'=8] {'tp'}, dimensions={0} | all-to-all | bytes 4194304 | tf_op jit(solution)/shard_map/all_to_all | solution.py:74
  257.6 55.0 %all-gather.5.cloned.1.call-done = bf16[2048,2048]{1,0:T(8,128)(2,1)} async-done(((bf16[64,2048]{1,0:T(8,128)(2,1)}), bf16[2048,2048]{1,0:T(8,128)(2,1)}) %all-gather.5.cloned.1.call-update) | async-done | bytes 8388624 | tf_op jit(solution)/shard_map/all_gather | solution.py:17
  312.6 9.4 %fusion.4 = bf16[512,2048]{1,0:T(8,128)(2,1)} fusion(bf16[2048,2048]{1,0:T(8,128)(2,1)} %all-gather.5.cloned.1.call-done, bf16[512,2048]{1,0:T(8,128)(2,1)S(1)} %bitcast.124), kind=kOutput, calls=%fused_computation.9 | convolution fusion | flops 4297588736 | bytes 12582912 | tf_op jit(solution)/shard_map/dot_general | solution.py:200
  322.0 51.1 %all_to_all.17 = bf16[8,64,2048]{2,1,0:T(8,128)(2,1)S(1)} all-to-all(bf16[8,64,2048]{2,1,0:T(8,128)(2,1)} %bitcast.125), channel_id=1, replica_groups=mesh['grp'=2,'sp'=32,'tp'=8] {'tp'}, dimensions={0} | all-to-all | bytes 4194304 | tf_op jit(solution)/shard_map/all_to_all | solution.py:62
  373.0 0.4 convert_reduce_fusion
  373.4 0.8 fusion.18
  (8 shorter events, 0.1 us)
Async XLA Ops:
  6.5 167.0 %copy-start = (bf16[128,2048]{1,0:T(8,128)(2,1)S(1)}, bf16[128,2048]{1,0:T(8,128)(2,1)}, u32[]{:S(2)}) copy-start(bf16[128,2048]{1,0:T(8,128)(2,1)} %param.23) | copy-start | bytes 1572868
  6.6 20.6 %copy-start.6 = (f32[1,512]{1,0:T(1,128)S(1)}, f32[1,512]{1,0:T(1,128)}, u32[]{:S(2)}) copy-start(f32[1,512]{1,0:T(1,128)} %param.19) | copy-start | bytes 6148
  6.6 159.9 %all-gather.7.cloned.1.call-start = ((), (), s32[]{:S(2)}) async-start(), calls=%async_computation.4 | async-start | bytes 2297856 | tf_op jit(solution)/shard_map/all_gather | solution.py:33
  25.2 287.4 %all-gather.5.cloned.1.call-start = ((), (), s32[]{:S(2)}) async-start(), calls=%async_computation.3 | async-start | bytes 8650752 | tf_op jit(solution)/shard_map/all_gather | solution.py:17
  27.0 139.4 %copy-start.4 = (pred[128,128]{0,1:T(8,128)(4,1)}, pred[128,128]{0,1:T(8,128)(4,1)S(1)}, u32[]{:S(2)}) copy-start(pred[128,128]{0,1:T(8,128)(4,1)S(1)} %iota_compare_fusion) | copy-start | bytes 49156
  168.2 3.2 copy-start.2
  169.9 2.5 copy-start.1
  170.0 3.4 copy-start.8
  170.0 3.4 copy-start.5
  226.3 1.0 copy-start.3
  226.4 1.1 copy-start.7
Sparse Core Ops, SparseCore 0:
  25.3 141.1 all-gather.6
  168.5 144.0 all-gather.4
where the time goes:
time: 385 us; the launch traced here: 381 us
  waiting for transfers between devices  194 us (50%)
  blocking collectives  133 us (35%)
  between operations  25 us (6%)
  matrix products  13.7 us (4%)
  other arithmetic  9.31 us (2%)
  local copies, waits for them, and re-layouts  5.93 us (2%)
    all_gather x1, waiting for transfers between devices, all_in_one(): both, at, found = (lax.all_gather(jnp.concatenate(lines), axis), 0, {})  139 us
    all_to_all x2, blocking collectives, sum_at_owner(): blocks = lax.all_to_all(cut_along(x, dim, length), axis, 0, 0, tiled=True)  103 us
    all_gather x1, waiting for transfers between devices, turned_gather(): filled, at, outs = (lax.all_gather(both, axis, axis=0, tiled=True), 0, [])  55 us
    all_to_all x1, blocking collectives, copy_for_each(): return lax.all_to_all(copies, axis, split_axis=0, concat_axis=0, tiled=True)  29.7 us
    dot_general x1, matrix products, shards(): jnp.dot(active, whole_down, preferred_element_type=jnp.float32)  9.37 us
  transfers between devices with their start and end apart: 2, of which 2 were waited for; matrix products, arithmetic and copies ran while one was open for 2% of the time, Pallas kernels for 0%

commit v1 on v0

--- a/solution.py
+++ b/solution.py
@@ -22,34 +22,34 @@
     return tuple(outs)
 
 
-def all_in_one(x, axis):
-    leaves = jax.tree.leaves(x)
-    order = sorted(range(len(leaves)), key=lambda k: -leaves[k].size)
-    width = (1, *leaves[order[0]].shape)[-1]
-    lines = [
-        jnp.pad(leaves[k].reshape(-1), (0, -leaves[k].size % width)).reshape(-1, width)
-        for k in order
-    ]
-    both, at, found = (lax.all_gather(jnp.concatenate(lines), axis), 0, {})
-    for k, line in zip(order, lines):
-        piece = both[:, at : at + len(line)].reshape(len(both), -1)
-        found[k] = piece[:, : leaves[k].size].reshape(-1, *leaves[k].shape)
-        at += len(line)
-    numbers = iter(range(len(leaves)))
-    return jax.tree.map(lambda _: found[next(numbers)], x)
-
-
-def prefix_2(part, axis, combine, identity):
+def shifted_on(x, axis, distance):
+    length = lax.axis_size(axis)
+    return lax.ppermute(x, axis, [(k, k + distance) for k in range(length - distance)])
+
+
+def packed(state):
+    total, top, memory = state
+    scalars = jnp.stack([total, top], axis=1)
+    row = jnp.pad(scalars, ((0, 0), (0, memory.shape[-1] - 2)))
+    return jnp.concatenate([memory, jnp.broadcast_to(row[:, None], (*row.shape[:1], 8, row.shape[1]))], axis=1)
+
+
+def unpacked(both, head_dim, present):
+    top = jnp.where(present, both[:, head_dim, 1], neg_big)
+    return (both[:, head_dim, 0], top, both[:, :head_dim])
+
+
+def prefix_by_doubling(part, axis, combine):
     place = lax.axis_index(axis)
-    gathered = all_in_one(part, axis)
-    state = jax.tree.map(lambda a, e: jnp.zeros_like(a) + jnp.asarray(e, a.dtype), part, identity)
-
-    def one(step, state):
-        return combine(
-            state, jax.tree.map(lambda a: lax.dynamic_index_in_dim(a, step, 0, False), gathered)
-        )
-
-    return lax.fori_loop(0, place, one, state)
+    length = lax.axis_size(axis)
+    head_dim = part[2].shape[-1]
+    window, earlier, distance = (part, None, 1)
+    while distance < length:
+        found = unpacked(shifted_on(packed(window), axis, distance), head_dim, place >= distance)
+        earlier = found if earlier is None else combine(found, earlier)
+        window = combine(found, window)
+        distance *= 2
+    return earlier
 
 
 def cut_along(x, dim, length):
@@ -156,7 +156,7 @@
     for block_idx in range(block_count):
         prefixes.append(running)
         running = combine(running, tuple((member[block_idx] for member in summaries)))
-    before = prefix_2(running, "sp", combine, zero_state)
+    before = prefix_by_doubling(running, "sp", combine)
     anchor = (zero_heads, zero_heads, zero_memory)
     incoming = combine(anchor, before)
     starts = [combine(incoming, prefix) for prefix in prefixes]

time: 385 us -> 259 us (0.67)
  waiting for transfers between devices: 194 us -> 6.46 us
  starting transfers between devices: 0.07 us -> 90.6 us
  blocking collectives: 133 us -> 98.2 us
  between operations: 25 us -> 35.4 us
    all_gather x1 -> x0, waiting for transfers between devices: 139 us -> none  [all_in_one(): both, at, found = (lax.all_gather(jnp.concatenate(lines), axis), 0, {})]
    ppermute x0 -> x5, starting transfers between devices: none -> 90.6 us  [shifted_on(): lax.ppermute(x, axis, [(k, k + distance) for k in range(length - distance)])]
    all_gather x1, waiting for transfers between devices: 55 us -> 0.01 us  [turned_gather(): filled, at, outs = (lax.all_gather(both, axis, axis=0, tiled=True), 0, [])]
    all_to_all x2, blocking collectives: 103 us -> 68.5 us  [sum_at_owner(): blocks = lax.all_to_all(cut_along(x, dim, length), axis, 0, 0, tiled=True)]
    ppermute x0 -> x5, waiting for transfers between devices: none -> 6.4 us  [shifted_on(): lax.ppermute(x, axis, [(k, k + distance) for k in range(length - distance)])]
  transfers between devices with their start and end apart: 2 -> 6, of which waited for: 2 -> 4; matrix products, arithmetic and copies ran while one was open for 2% -> 6% of each run, Pallas kernels for 0% -> 0%
where the time goes in v1:
time: 259 us; the launch traced here: 258 us
  blocking collectives  98.2 us (38%)
  starting transfers between devices  90.6 us (35%)
  between operations  35.4 us (14%)
  matrix products  12.9 us (5%)
  other arithmetic  9.23 us (4%)
  waiting for transfers between devices  6.46 us (2%)
  local copies, waits for them, and re-layouts  5.48 us (2%)
    ppermute x5, starting transfers between devices, shifted_on(): lax.ppermute(x, axis, [(k, k + distance) for k in range(length - distance)])  90.6 us
    all_to_all x2, blocking collectives, sum_at_owner(): blocks = lax.all_to_all(cut_along(x, dim, length), axis, 0, 0, tiled=True)  68.5 us
    all_to_all x1, blocking collectives, copy_for_each(): return lax.all_to_all(copies, axis, split_axis=0, concat_axis=0, tiled=True)  29.7 us
    dot_general x1, matrix products, shards(): jnp.dot(active, whole_down, preferred_element_type=jnp.float32)  9.37 us
    ppermute x5, waiting for transfers between devices, shifted_on(): lax.ppermute(x, axis, [(k, k + distance) for k in range(length - distance)])  6.4 us
  transfers between devices with their start and end apart: 6, of which 4 were waited for; matrix products, arithmetic and copies ran while one was open for 6% of the time, Pallas kernels for 0%

profile of v1, /device:TPU:33, one launch (start us, length us, event | category | flops | bytes accessed | tf_op | source)
XLA Modules:
  0.0 258.3 jit_solution(8656947608459289811)
XLA Ops:
  6.5 0.0 copy-start
  6.6 0.0 all-gather.2.cloned.1.call-start
  6.6 1.8 pad_maximum_fusion
  8.3 0.1 all-gather.2.cloned.1.call-update
  8.4 0.7 fusion.42
  9.1 1.2 reduce_window_sum.11
  10.3 0.7 fusion.57
  11.7 0.2 slice_reduce_fusion
  11.8 0.9 fusion.41
  12.7 0.7 fusion.58
  23.4 0.1 fusion.47
  23.4 0.8 subtract_exponential_fusion.1
  24.2 1.0 convert_multiply_fusion.2
  25.2 1.6 fusion.28
  26.8 0.0 copy-start.1
  26.9 5.3 %collective-permute-start = (f32[1,136,128]{2,1,0:T(8,128)S(1)}, f32[1,136,128]{2,1,0:T(8,128)S(1)}, u32[]{:S(2)}, u32[]{:S(2)}) collective-permute-start(f32[1,136,128]{2,1,0:T(8,128)S(1)} %pad_maximum_fusion.1), channel_id=1, source_target_pairs={{0,8},{8,16},{16,24},{24,32},{32,40},{40,48},{48,56},{56,64},{64,7... | collective-permute-start | bytes 208904 | tf_op jit(solution)/shard_map/ppermute | solution.py:27
  32.1 1.3 collective-permute-done
  33.5 0.7 fusion.56
  35.5 0.1 fusion.46
  35.6 6.6 %collective-permute-start.1 = (f32[1,136,128]{2,1,0:T(8,128)S(1)}, f32[1,136,128]{2,1,0:T(8,128)S(1)}, u32[]{:S(2)}, u32[]{:S(2)}) collective-permute-start(f32[1,136,128]{2,1,0:T(8,128)S(1)} %pad_maximum_fusion.2), channel_id=1, source_target_pairs={{0,16},{8,24},{16,32},{24,40},{32,48},{40,56},{48,64},{56,72},{64,... | collective-permute-start | bytes 208904 | tf_op jit(solution)/shard_map/ppermute | solution.py:27
  42.3 1.3 collective-permute-done.1
  43.7 0.6 fusion.55
  45.5 0.1 fusion.45
  45.7 12.8 %collective-permute-start.2 = (f32[1,136,128]{2,1,0:T(8,128)S(1)}, f32[1,136,128]{2,1,0:T(8,128)S(1)}, u32[]{:S(2)}, u32[]{:S(2)}) collective-permute-start(f32[1,136,128]{2,1,0:T(8,128)S(1)} %pad_maximum_fusion.3), channel_id=1, source_target_pairs={{0,32},{8,40},{16,48},{24,56},{32,64},{40,72},{48,80},{56,88},{64,... | collective-permute-start | bytes 208904 | tf_op jit(solution)/shard_map/ppermute | solution.py:27
  58.5 1.3 collective-permute-done.2
  59.8 0.6 fusion.54
  61.7 0.0 copy-start.4
  61.7 0.0 copy-start.7
  61.7 0.1 fusion.44
  61.8 27.1 %collective-permute-start.3 = (f32[1,136,128]{2,1,0:T(8,128)S(1)}, f32[1,136,128]{2,1,0:T(8,128)S(1)}, u32[]{:S(2)}, u32[]{:S(2)}) collective-permute-start(f32[1,136,128]{2,1,0:T(8,128)S(1)} %pad_maximum_fusion.4), channel_id=1, source_target_pairs={{0,64},{8,72},{16,80},{24,88},{32,96},{40,104},{48,112},{56,120},{... | collective-permute-start | bytes 208904 | tf_op jit(solution)/shard_map/ppermute | solution.py:27
  88.9 0.1 copy.19
  89.0 2.4 collective-permute-done.3
  91.4 0.6 fusion.53
  93.2 0.1 fusion.43
  93.3 38.8 %collective-permute-start.4 = (f32[1,136,128]{2,1,0:T(8,128)S(1)}, f32[1,136,128]{2,1,0:T(8,128)S(1)}, u32[]{:S(2)}, u32[]{:S(2)}) collective-permute-start(f32[1,136,128]{2,1,0:T(8,128)S(1)} %pad_maximum_fusion.5), channel_id=1, source_target_pairs={{0,128},{8,136},{16,144},{24,152},{32,160},{40,168},{48,176},{56,1... | collective-permute-start | bytes 208904 | tf_op jit(solution)/shard_map/ppermute | solution.py:27
  132.1 0.0 copy-done.5
  132.2 0.2 select_reduce_fusion
  135.7 0.0 collective-permute-done.4
  135.7 0.6 fusion.52
  138.7 0.1 maximum_bitcast_fusion.2
  138.8 0.1 subtract_exponential_fusion
  138.9 0.1 add_bitcast_fusion.3
  139.0 0.0 copy-done.2
  139.0 0.4 fusion.13
  139.4 0.0 copy-done.1
  139.4 0.4 fusion.59
  139.8 0.5 multiply_reduce_fusion
  140.3 0.0 copy-done.4
  140.3 0.0 copy-done.7
  140.3 0.1 fusion.27
  140.5 0.0 copy-done
  140.5 0.7 convolution_convert_fusion
  141.2 31.2 %all_to_all.15 = bf16[8,64,2048]{2,1,0:T(8,128)(2,1)S(1)} all-to-all(bf16[8,64,2048]{2,1,0:T(8,128)(2,1)S(1)} %bitcast.136), channel_id=1, replica_groups=mesh['grp'=2,'sp'=32,'tp'=8] {'tp'}, dimensions={0} | all-to-all | bytes 4194304 | tf_op jit(solution)/shard_map/all_to_all | solution.py:62
  172.4 0.4 convert_reduce_fusion.1
  172.7 0.6 copy-done.3
  173.3 0.2 fusion.15
  173.5 0.0 copy-done.6
  173.5 0.1 fusion.17
  173.7 0.2 broadcast_in_dim.52
  173.9 29.7 %all_to_all.16 = bf16[8,64,2048]{2,1,0:T(8,128)(2,1)S(1)} all-to-all(bf16[8,64,2048]{2,1,0:T(8,128)(2,1)S(1)} %broadcast_in_dim.52), channel_id=1, replica_groups=mesh['grp'=2,'sp'=32,'tp'=8] {'tp'}, dimensions={0} | all-to-all | bytes 4194304 | tf_op jit(solution)/shard_map/all_to_all | solution.py:74
  203.6 9.4 %fusion.4 = bf16[512,2048]{1,0:T(8,128)(2,1)} fusion(bf16[2048,2048]{1,0:T(8,128)(2,1)} %all-gather.2.cloned.1.call-done, bf16[512,2048]{1,0:T(8,128)(2,1)S(1)} %bitcast.139), kind=kOutput, calls=%fused_computation.6 | convolution fusion | flops 4297588736 | bytes 12582912 | tf_op jit(solution)/shard_map/dot_general | solution.py:200
  213.0 37.3 %all_to_all.17 = bf16[8,64,2048]{2,1,0:T(8,128)(2,1)S(1)} all-to-all(bf16[8,64,2048]{2,1,0:T(8,128)(2,1)} %bitcast.140), channel_id=1, replica_groups=mesh['grp'=2,'sp'=32,'tp'=8] {'tp'}, dimensions={0} | all-to-all | bytes 4194304 | tf_op jit(solution)/shard_map/all_to_all | solution.py:62
  250.3 0.4 convert_reduce_fusion
  250.7 0.8 fusion.18
  (24 shorter events, 0.2 us)
Async XLA Ops:
  6.5 133.9 %copy-start = (bf16[128,2048]{1,0:T(8,128)(2,1)S(1)}, bf16[128,2048]{1,0:T(8,128)(2,1)}, u32[]{:S(2)}) copy-start(bf16[128,2048]{1,0:T(8,128)(2,1)} %param.21) | copy-start | bytes 1572868
  6.6 125.6 %copy-start.5 = (f32[1,512]{1,0:T(1,128)S(1)}, f32[1,512]{1,0:T(1,128)}, u32[]{:S(2)}) copy-start(f32[1,512]{1,0:T(1,128)} %param.17) | copy-start | bytes 6148
  6.6 197.1 %all-gather.2.cloned.1.call-start = ((), (), s32[]{:S(2)}) async-start(), calls=%async_computation.3 | async-start | bytes 8650752 | tf_op jit(solution)/shard_map/all_gather | solution.py:17
  24.2 114.8 %copy-start.2 = (bf16[512,128]{1,0:T(8,128)(2,1)S(1)}, bf16[512,128]{1,0:T(8,128)(2,1)}, u32[]{:S(2)}) copy-start(bf16[512,128]{1,0:T(8,128)(2,1)} %param.13) | copy-start | bytes 393220
  26.8 112.6 %copy-start.1 = (bf16[512,128]{1,0:T(8,128)(2,1)S(1)}, bf16[512,128]{1,0:T(8,128)(2,1)}, u32[]{:S(2)}) copy-start(bf16[512,128]{1,0:T(8,128)(2,1)} %param.15) | copy-start | bytes 393220
  26.9 6.6 %collective-permute-start = (f32[1,136,128]{2,1,0:T(8,128)S(1)}, f32[1,136,128]{2,1,0:T(8,128)S(1)}, u32[]{:S(2)}, u32[]{:S(2)}) collective-permute-start(f32[1,136,128]{2,1,0:T(8,128)S(1)} %pad_maximum_fusion.1), channel_id=1, source_target_pairs={{0,8},{8,16},{16,24},{24,32},{32,40},{40,48},{48,56},{56,64},{64,7... | collective-permute-start | bytes 208904 | tf_op jit(solution)/shard_map/ppermute | solution.py:27
  35.6 8.0 %collective-permute-start.1 = (f32[1,136,128]{2,1,0:T(8,128)S(1)}, f32[1,136,128]{2,1,0:T(8,128)S(1)}, u32[]{:S(2)}, u32[]{:S(2)}) collective-permute-start(f32[1,136,128]{2,1,0:T(8,128)S(1)} %pad_maximum_fusion.2), channel_id=1, source_target_pairs={{0,16},{8,24},{16,32},{24,40},{32,48},{40,56},{48,64},{56,72},{64,... | collective-permute-start | bytes 208904 | tf_op jit(solution)/shard_map/ppermute | solution.py:27
  45.7 14.2 %collective-permute-start.2 = (f32[1,136,128]{2,1,0:T(8,128)S(1)}, f32[1,136,128]{2,1,0:T(8,128)S(1)}, u32[]{:S(2)}, u32[]{:S(2)}) collective-permute-start(f32[1,136,128]{2,1,0:T(8,128)S(1)} %pad_maximum_fusion.3), channel_id=1, source_target_pairs={{0,32},{8,40},{16,48},{24,56},{32,64},{40,72},{48,80},{56,88},{64,... | collective-permute-start | bytes 208904 | tf_op jit(solution)/shard_map/ppermute | solution.py:27
  61.7 78.6 %copy-start.4 = (bf16[512,128]{1,0:T(8,128)(2,1)S(1)}, bf16[512,128]{1,0:T(8,128)(2,1)}, u32[]{:S(2)}) copy-start(bf16[512,128]{1,0:T(8,128)(2,1)} %param.16) | copy-start | bytes 393220
  61.7 78.6 %copy-start.7 = (f32[128]{0:T(128)S(1)}, f32[128]{0:T(128)}, u32[]{:S(2)}) copy-start(f32[128]{0:T(128)} %param.20) | copy-start | bytes 1540
  61.8 29.6 %collective-permute-start.3 = (f32[1,136,128]{2,1,0:T(8,128)S(1)}, f32[1,136,128]{2,1,0:T(8,128)S(1)}, u32[]{:S(2)}, u32[]{:S(2)}) collective-permute-start(f32[1,136,128]{2,1,0:T(8,128)S(1)} %pad_maximum_fusion.4), channel_id=1, source_target_pairs={{0,64},{8,72},{16,80},{24,88},{32,96},{40,104},{48,112},{56,120},{... | collective-permute-start | bytes 208904 | tf_op jit(solution)/shard_map/ppermute | solution.py:27
  93.3 42.4 %collective-permute-start.4 = (f32[1,136,128]{2,1,0:T(8,128)S(1)}, f32[1,136,128]{2,1,0:T(8,128)S(1)}, u32[]{:S(2)}, u32[]{:S(2)}) collective-permute-start(f32[1,136,128]{2,1,0:T(8,128)S(1)} %pad_maximum_fusion.5), channel_id=1, source_target_pairs={{0,128},{8,136},{16,144},{24,152},{32,160},{40,168},{48,176},{56,1... | collective-permute-start | bytes 208904 | tf_op jit(solution)/shard_map/ppermute | solution.py:27
  172.4 1.0 copy-start.3
  172.4 1.2 copy-start.6
Sparse Core Ops, SparseCore 0:
  9.4 186.2 all-gather.1

commit v2 on v1

v2 whole, which is shorter than its diff:
```python
import jax
import jax.numpy as jnp
from jax import lax
from jax.experimental import pallas as pl
from jax.experimental.pallas import tpu as pltpu
from jax.sharding import PartitionSpec as P

BLOCK = 128


neg_big = -1e30
norm_eps = 1e-06
highest = lax.Precision.HIGHEST


def gathered_weights(up, down, axis):
    return lax.all_gather(jnp.concatenate([up, down.T], axis=1), axis, axis=0, tiled=True)


def shifted_on(x, axis, distance):
    length = lax.axis_size(axis)
    return lax.ppermute(x, axis, [(k, k + distance) for k in range(length - distance)])


def bf16_parts(x):
    parts = []
    for _ in range(3):
        part = lax.reduce_precision(x, 8, 7)
        parts.append(part.astype(jnp.bfloat16))
        x = x - part
    return parts


def packed(state):
    total, top, memory = state
    rows = bf16_parts(total) + bf16_parts(top)
    rows = jnp.concatenate(rows, axis=1)
    rows = jnp.pad(rows, ((0, 0), (0, 16 - rows.shape[1]), (0, 0)))
    return jnp.concatenate([memory.astype(jnp.bfloat16), rows], axis=1)


def unpacked(both, head_dim, present):
    both = both.astype(jnp.float32)
    total = jnp.sum(both[:, head_dim : head_dim + 3], axis=1, keepdims=True)
    top = jnp.sum(both[:, head_dim + 3 : head_dim + 6], axis=1, keepdims=True)
    return (total, jnp.where(present, top, neg_big), both[:, :head_dim])


def prefix_by_doubling(part, axis):
    place = lax.axis_index(axis)
    length = lax.axis_size(axis)
    head_dim = part[2].shape[-1]
    window, earlier, distance = (part, None, 1)
    while distance < length:
        found = unpacked(shifted_on(packed(window), axis, distance), head_dim, place >= distance)
        earlier = found if earlier is None else combine(found, earlier)
        window = combine(found, window)
        distance *= 2
    return earlier


def turned_by(x, axis, steps):
    length = lax.axis_size(axis)
    return lax.ppermute(x, axis, [(k, (k + steps) % length) for k in range(length)])


def with_partner(x, axis):
    return lax.ppermute(x, axis, [(k, k ^ 1) for k in range(lax.axis_size(axis))])


def in_relative_order(x, axis):
    chips = lax.axis_size(axis) // 2
    place = lax.axis_index(axis)
    chip, core = (place // 2, place % 2)
    blocks = x.reshape(chips, 2, -1, x.shape[-1])
    blocks = jnp.where(core == 0, blocks, blocks[:, ::-1])
    rows = [
        lax.dynamic_index_in_dim(blocks, (chip - d + chips) % chips, 0, False) for d in range(chips)
    ]
    return jnp.concatenate([r[0] for r in rows] + [r[1] for r in rows], axis=0)


def sum_of_relative_rows(kept, sent, axis):
    chips = lax.axis_size(axis) // 2
    found = with_partner(sent, axis)
    both = (kept.astype(jnp.float32) + found.astype(jnp.float32)).astype(jnp.bfloat16)
    blocks = both.reshape(chips, -1, both.shape[-1])
    arrived = {d: turned_by(blocks[d], axis, -2 * d) for d in (2, 1, 3)}
    total = blocks[0].astype(jnp.float32)
    for d in range(1, chips):
        total = total + arrived[d].astype(jnp.float32)
    return total


def relative_rows(x, axis):
    chips = lax.axis_size(axis) // 2
    found = {d: turned_by(x, axis, 2 * d) for d in (2, 1, 3)}
    own = jnp.concatenate([x] + [found[d] for d in range(1, chips)], axis=0)
    return own, with_partner(own, axis)


def rms_norm(tensor, gain_vec):
    mean_sq = jnp.mean(tensor * tensor, axis=-1, keepdims=True)
    return tensor * lax.rsqrt(mean_sq + norm_eps) * gain_vec


def combine(earlier, later):
    total_e, max_e, memory_e = earlier
    total_l, max_l, memory_l = later
    carried = total_l + max_e
    new_max = jnp.maximum(carried, max_l)
    old_part = jnp.exp(carried - new_max)
    new_part = jnp.exp(max_l - new_max)
    return (total_e + total_l, new_max, old_part * memory_e + new_part * memory_l)


def block_prefixes(totals, tops, memories):
    count = totals.shape[0]
    j = lax.broadcasted_iota(jnp.int32, (count + 1, count, count), 0)
    b = lax.broadcasted_iota(jnp.int32, (count + 1, count, count), 1)
    i = lax.broadcasted_iota(jnp.int32, (count + 1, count, count), 2)
    between = ((b < i) & (i < j))[..., None]
    gap = jnp.sum(jnp.where(between, totals[None, None], 0.0), axis=2)
    used = (b < j)[:, :, :1]
    logs = jnp.where(used, gap + tops[None], neg_big)
    top = jnp.max(logs, axis=1)
    scale = jnp.where(used, jnp.exp(logs - top[:, None]), 0.0)
    total = jnp.sum(jnp.where(used, totals[None], 0.0), axis=1)
    memory = jnp.sum(scale[..., None, None] * memories[None], axis=1)
    lanes = (count + 1, totals.shape[1], 1, memories.shape[-1])
    spread = lambda x: jnp.broadcast_to(x[..., None, None], lanes)
    return spread(total), spread(top), memory


def feed_forward_kernel(own_ref, other_ref, up_ref, down_ref, out_ref, active_ref):
    step = pl.program_id(0)
    width = up_ref.shape[1]
    ups = active_ref.shape[1] // width
    half = own_ref.shape[0]

    @pl.when(step < ups)
    def _():
        cols = pl.ds(pl.multiple_of(step * width, width), width)
        for k, rows_ref in enumerate((own_ref, other_ref)):
            upward = jnp.dot(rows_ref[...], up_ref[...], preferred_element_type=jnp.float32)
            active = jnp.square(jnp.maximum(upward, 0.0)).astype(jnp.bfloat16)
            active_ref[k * half : (k + 1) * half, cols] = active

    @pl.when(step >= ups)
    def _():
        out_ref[...] = lax.dot_general(
            active_ref[...],
            down_ref[...],
            (((1,), (1,)), ((), ())),
            preferred_element_type=jnp.float32,
        ).astype(jnp.bfloat16)


def feed_forward(own, other, weights, hidden):
    half, features = own.shape
    up_width, down_height = (hidden // 2, features // 4)
    ups, downs = (hidden // up_width, features // down_height)
    return pl.pallas_call(
        feed_forward_kernel,
        grid=(ups + downs,),
        out_shape=jax.ShapeDtypeStruct((2 * half, features), jnp.bfloat16),
        in_specs=[
            pl.BlockSpec((half, features), lambda i: (0, 0)),
            pl.BlockSpec((half, features), lambda i: (0, 0)),
            pl.BlockSpec((features, up_width), lambda i: (0, jnp.minimum(i, ups - 1))),
            pl.BlockSpec((down_height, hidden), lambda i: (jnp.maximum(i - ups, 0), 1)),
        ],
        out_specs=pl.BlockSpec((2 * half, down_height), lambda i: (0, jnp.maximum(i - ups, 0))),
        scratch_shapes=[pltpu.VMEM((2 * half, hidden), jnp.bfloat16)],
        compiler_params=pltpu.CompilerParams(
            dimension_semantics=("arbitrary",), vmem_limit_bytes=40 * 1024 * 1024
        ),
        cost_estimate=pl.CostEstimate(
            flops=8 * half * features * hidden,
            bytes_accessed=4 * features * hidden + 8 * half * features,
            transcendentals=0,
        ),
        name="feed_forward",
    )(own, other, weights, weights)


def block_summary(key_blk, val_blk, gate_blk, decay_logarithm):
    block_total = decay_logarithm[..., -1]
    tail_log = block_total[..., None] - decay_logarithm + gate_blk
    tail_max = jnp.max(tail_log, axis=-1)
    weights = jnp.exp(tail_log - tail_max[..., None])
    memory = jnp.einsum("bhsv,bhsk->bhvk", weights[..., None] * val_blk, key_blk, precision=highest)
    return (block_total, tail_max, memory)


def shards(
    queries,
    memory_keys,
    memory_values,
    output_preactivation,
    input_preactivation,
    forget_preactivation,
    extra_forget_terms,
    head_norm_gain,
    output_projection_matrix,
    residual,
    feedforward_norm_gain,
    feedforward_up_matrix,
    feedforward_down_matrix,
):
    tok_count = queries.shape[0]
    head_count = input_preactivation.shape[0]
    head_dim = queries.shape[1] // head_count
    block_len = BLOCK
    block_count = tok_count // block_len
    weights = gathered_weights(feedforward_up_matrix, feedforward_down_matrix, "sp")

    def to_blocks(tensor):
        return (
            tensor.astype(jnp.float32)
            .reshape(block_count, block_len, head_count, head_dim)
            .transpose(0, 2, 1, 3)
        )

    def gate_block_list(tensor):
        return tensor.reshape(head_count, block_count, block_len).transpose(1, 0, 2)

    query_blk = to_blocks(queries)
    key_blk = to_blocks(memory_keys) * head_dim ** (-0.5)
    val_blk = to_blocks(memory_values)
    gate_blk = gate_block_list(input_preactivation)
    decay_logarithm = jnp.cumsum(
        gate_block_list(jax.nn.log_sigmoid(forget_preactivation) + extra_forget_terms), axis=-1
    )
    summaries = block_summary(key_blk, val_blk, gate_blk, decay_logarithm)
    prefix_total, prefix_top, prefix_memory = block_prefixes(*summaries)
    whole = (prefix_total[-1], prefix_top[-1], prefix_memory[-1])
    before_total, before_top, before_memory = prefix_by_doubling(whole, "sp")
    incoming_top = jnp.maximum(before_total, before_top)
    incoming_memory = jnp.exp(before_top - incoming_top) * before_memory
    carried = prefix_total[:-1] + incoming_top
    start_top = jnp.maximum(carried, prefix_top[:-1])
    start_memory = (
        jnp.exp(carried - start_top) * incoming_memory
        + jnp.exp(prefix_top[:-1] - start_top) * prefix_memory[:-1]
    )
    start_max = start_top[:, :, 0, 0]
    causal = lax.broadcasted_iota(jnp.int32, (block_len, block_len), 0) >= lax.broadcasted_iota(
        jnp.int32, (block_len, block_len), 1
    )
    log_weight = (
        decay_logarithm[..., :, None] - decay_logarithm[..., None, :] + gate_blk[..., None, :]
    )
    log_weight = jnp.where(causal, log_weight, neg_big)
    carry_log = decay_logarithm + start_max[..., None]
    row_max = jnp.maximum(jnp.max(log_weight, axis=-1), carry_log)
    scores = jnp.einsum("bhtd,bhsd->bhts", query_blk, key_blk, precision=highest) * jnp.exp(
        log_weight - row_max[..., None]
    )
    carry_scale = jnp.exp(carry_log - row_max)
    hidden = jnp.einsum("bhts,bhsv->bhtv", scores, val_blk, precision=highest)
    hidden = hidden + carry_scale[..., None] * jnp.einsum(
        "bhvk,bhtk->bhtv", start_memory, query_blk, precision=highest
    )
    hidden = hidden.transpose(0, 2, 1, 3).reshape(tok_count, head_count, head_dim)
    gated = rms_norm(hidden, head_norm_gain) * jax.nn.sigmoid(
        output_preactivation.astype(jnp.float32).reshape(tok_count, head_count, head_dim)
    )
    mixed = gated.reshape(tok_count, head_count * head_dim).astype(jnp.bfloat16)
    mixed = in_relative_order(mixed, "tp")
    partial_branch = jnp.dot(
        mixed, output_projection_matrix, preferred_element_type=jnp.float32
    ).astype(jnp.bfloat16)
    middle = tok_count // 2
    branch = sum_of_relative_rows(partial_branch[:middle], partial_branch[middle:], "tp")
    mid_state = (residual.astype(jnp.float32) + branch).astype(jnp.bfloat16)
    normed = rms_norm(mid_state.astype(jnp.float32), feedforward_norm_gain).astype(jnp.bfloat16)
    own, other = relative_rows(normed, "tp")
    mlp_rows = feed_forward(own, other, weights, feedforward_up_matrix.shape[1])
    mlp_sum = sum_of_relative_rows(mlp_rows[:middle], mlp_rows[middle:], "tp")
    return (mid_state.astype(jnp.float32) + mlp_sum).astype(jnp.bfloat16)


def solution(mesh):
    in_specs = (
        P(("grp", "sp"), "tp"),
        P(("grp", "sp"), "tp"),
        P(("grp", "sp"), "tp"),
        P(("grp", "sp"), "tp"),
        P("tp", ("grp", "sp")),
        P("tp", ("grp", "sp")),
        P("tp", ("grp", "sp")),
        P(),
        P("tp", None),
        P(("grp", "sp", "tp"), None),
        P(),
        P("sp", "tp"),
        P("tp", "sp"),
    )
    out_specs = P(("grp", "sp", "tp"), None)
    return jax.shard_map(shards, mesh=mesh, in_specs=in_specs, out_specs=out_specs, check_vma=False)
```

time: 259 us -> 241 us (0.931)
  blocking collectives: 98.2 us -> 0 us
  starting transfers between devices: 90.6 us -> 136 us
  waiting for transfers between devices: 6.46 us -> 48.5 us
  between operations: 35.4 us -> 25 us
  matrix products: 12.9 us -> 3.63 us
  Pallas kernels: 0 us -> 6.42 us
  other arithmetic: 9.23 us -> 12.5 us
    all_to_all x3 -> x0, blocking collectives: 98.2 us -> none  [the longest x2 68.5 us: sum_at_owner(): blocks = lax.all_to_all(cut_along(x, dim, length), axis, 0, 0, tiled=True)]
    ppermute x0 -> x12, starting transfers between devices: none -> 55.7 us  [the longest x3 28.5 us: with_partner(): lax.ppermute(x, axis, [(k, k ^ 1) for k in range(lax.axis_size(axis))])]
    ppermute x0 -> x12, waiting for transfers between devices: none -> 38.5 us  [the longest x9 31.7 us: turned_by(): lax.ppermute(x, axis, [(k, (k + steps) % length) for k in range(length)])]
    ppermute x5, starting transfers between devices: 90.6 us -> 80.7 us  [shifted_on(): lax.ppermute(x, axis, [(k, k + distance) for k in range(length - distance)])]
    dot_general x1 -> x0, matrix products: 9.37 us -> none  [shards(): jnp.dot(active, whole_down, preferred_element_type=jnp.float32)]
    pallas_call x0 -> x1, Pallas kernels: none -> 6.42 us  [feed_forward(): pl.pallas_call(feed_forward_kernel, grid=(ups + downs,), out_shape=jax.Sh...]
    all_gather x1, waiting for transfers between devices: 0.01 us -> 4.84 us  [gathered_weights(): lax.all_gather(jnp.concatenate([up, down.T], axis=1), axis, axis=0, tiled...]
    unnamed x16 -> x25, local copies, waits for them, and re-layouts: 0.63 us -> 3.54 us
  transfers between devices with their start and end apart: 6 -> 18, of which waited for: 4 -> 15; matrix products, arithmetic and copies ran while one was open for 6% -> 7% of each run, Pallas kernels for 0% -> 0%
where the time goes in v2:
time: 241 us; the launch traced here: 239 us
  starting transfers between devices  136 us (56%)
  waiting for transfers between devices  48.5 us (20%)
  between operations  25 us (10%)
  other arithmetic  12.5 us (5%)
  local copies, waits for them, and re-layouts  6.95 us (3%)
  Pallas kernels  6.42 us (3%)
  matrix products  3.63 us (2%)
    ppermute x5, starting transfers between devices, shifted_on(): lax.ppermute(x, axis, [(k, k + distance) for k in range(length - distance)])  80.7 us
    ppermute x9, waiting for transfers between devices, turned_by(): lax.ppermute(x, axis, [(k, (k + steps) % length) for k in range(length)])  31.7 us
    ppermute x3, starting transfers between devices, with_partner(): lax.ppermute(x, axis, [(k, k ^ 1) for k in range(lax.axis_size(axis))])  28.5 us
    ppermute x9, starting transfers between devices, turned_by(): lax.ppermute(x, axis, [(k, (k + steps) % length) for k in range(length)])  27.2 us
    ppermute x3, waiting for transfers between devices, with_partner(): lax.ppermute(x, axis, [(k, k ^ 1) for k in range(lax.axis_size(axis))])  6.79 us
    pallas_call x1, Pallas kernels, feed_forward(): pl.pallas_call(feed_forward_kernel, grid=(ups + downs,), out_shape=jax.Sh...  6.42 us
    ppermute x5, waiting for transfers between devices, shifted_on(): lax.ppermute(x, axis, [(k, k + distance) for k in range(length - distance)])  5.13 us
    all_gather x1, waiting for transfers between devices, gathered_weights(): lax.all_gather(jnp.concatenate([up, down.T], axis=1), axis, axis=0, tiled...  4.84 us
  transfers between devices with their start and end apart: 18, of which 15 were waited for; matrix products, arithmetic and copies ran while one was open for 7% of the time, Pallas kernels for 0%

profile of v2, /device:TPU:33, one launch (start us, length us, event | category | flops | bytes accessed | tf_op | source)
XLA Modules:
  0.0 239.4 jit_solution(14544904261256703616)
XLA Ops:
  6.6 1.7 pad_maximum_fusion.1
  8.4 0.7 fusion.45
  9.1 1.2 reduce_window_sum.11
  10.3 0.2 slice_reduce_fusion.10
  10.6 0.9 fusion.44
  11.7 0.6 slice.171
  17.0 0.6 slice.172
  23.7 0.8 subtract_exponential_fusion.1
  24.5 0.9 convert_multiply_fusion.2
  25.4 1.6 fusion.13
  27.1 0.2 multiply_reduce_fusion
  27.3 0.6 squeeze.62
  28.0 0.6 squeeze.65
  28.6 5.2 %collective-permute-start = (bf16[1,144,128]{2,1,0:T(8,128)(2,1)S(1)}, bf16[1,144,128]{2,1,0:T(8,128)(2,1)S(1)}, u32[]{:S(2)}, u32[]{:S(2)}) collective-permute-start(bf16[1,144,128]{2,1,0:T(8,128)(2,1)S(1)} %fusion.28), channel_id=1, source_target_pairs={{0,8},{8,16},{16,24},{24,32},{32,40},{40,48},{48,56},{56,64},{64,7... | collective-permute-start | bytes 110600 | tf_op jit(solution)/shard_map/ppermute | solution.py:22
  33.9 1.0 collective-permute-done
  35.0 0.6 fusion.48
  35.5 1.2 subtract_exponential_fusion.16
  36.8 0.6 subtract_exponential_fusion.15
  37.5 6.6 %collective-permute-start.1 = (bf16[1,144,128]{2,1,0:T(8,128)(2,1)S(1)}, bf16[1,144,128]{2,1,0:T(8,128)(2,1)S(1)}, u32[]{:S(2)}, u32[]{:S(2)}) collective-permute-start(bf16[1,144,128]{2,1,0:T(8,128)(2,1)S(1)} %fusion.29), channel_id=1, source_target_pairs={{0,16},{8,24},{16,32},{24,40},{32,48},{40,56},{48,64},{56,72},{64,... | collective-permute-start | bytes 110600 | tf_op jit(solution)/shard_map/ppermute | solution.py:22
  44.1 1.0 collective-permute-done.1
  45.4 12.5 %collective-permute-start.2 = (bf16[1,144,128]{2,1,0:T(8,128)(2,1)S(1)}, bf16[1,144,128]{2,1,0:T(8,128)(2,1)S(1)}, u32[]{:S(2)}, u32[]{:S(2)}) collective-permute-start(bf16[1,144,128]{2,1,0:T(8,128)(2,1)S(1)} %fusion.30), channel_id=1, source_target_pairs={{0,32},{8,40},{16,48},{24,56},{32,64},{40,72},{48,80},{56,88},{64,... | collective-permute-start | bytes 110600 | tf_op jit(solution)/shard_map/ppermute | solution.py:22
  57.9 1.0 collective-permute-done.2
  59.1 22.7 %collective-permute-start.3 = (bf16[1,144,128]{2,1,0:T(8,128)(2,1)S(1)}, bf16[1,144,128]{2,1,0:T(8,128)(2,1)S(1)}, u32[]{:S(2)}, u32[]{:S(2)}) collective-permute-start(bf16[1,144,128]{2,1,0:T(8,128)(2,1)S(1)} %fusion.31), channel_id=1, source_target_pairs={{0,64},{8,72},{16,80},{24,88},{32,96},{40,104},{48,112},{56,120},{... | collective-permute-start | bytes 110600 | tf_op jit(solution)/shard_map/ppermute | solution.py:22
  81.9 0.1 copy.31
  82.0 1.2 collective-permute-done.3
  83.3 33.6 %collective-permute-start.4 = (bf16[1,144,128]{2,1,0:T(8,128)(2,1)S(1)}, bf16[1,144,128]{2,1,0:T(8,128)(2,1)S(1)}, u32[]{:S(2)}, u32[]{:S(2)}) collective-permute-start(bf16[1,144,128]{2,1,0:T(8,128)(2,1)S(1)} %fusion.32), channel_id=1, source_target_pairs={{0,128},{8,136},{16,144},{24,152},{32,160},{40,168},{48,176},{56,1... | collective-permute-start | bytes 110600 | tf_op jit(solution)/shard_map/ppermute | solution.py:22
  116.9 0.2 select_reduce_fusion
  117.3 0.8 collective-permute-done.4
  118.2 0.1 slice_reduce_fusion.11
  118.6 0.4 fusion.2
  119.0 0.4 fusion.90
  119.4 0.5 multiply_reduce_fusion.1
  120.0 0.1 fusion.11
  120.3 0.7 convolution_convert_fusion
  121.0 0.1 slice.230
  121.1 6.5 %collective-permute-start.5 = (bf16[256,2048]{1,0:T(8,128)(2,1)S(1)}, bf16[256,2048]{1,0:T(8,128)(2,1)S(1)}, u32[]{:S(2)}, u32[]{:S(2)}) collective-permute-start(bf16[256,2048]{1,0:T(8,128)(2,1)S(1)} %slice.230), channel_id=1, source_target_pairs={{0,1},{1,0},{2,3},{3,2},{4,5},{5,4},{6,7},{7,6},{8,9},{9,8},{10,11... | collective-permute-start | bytes 3145736 | tf_op jit(solution)/shard_map/ppermute | solution.py:68
  127.7 2.3 collective-permute-done.5
  129.9 0.4 add_convert_fusion.1
  130.4 4.6 %collective-permute-start.6 = (bf16[64,2048]{1,0:T(8,128)(2,1)S(1)}, bf16[64,2048]{1,0:T(8,128)(2,1)S(1)}, u32[]{:S(2)}, u32[]{:S(2)}) collective-permute-start(bf16[64,2048]{1,0:T(8,128)(2,1)S(1)} %get-tuple-element.54), channel_id=1, source_target_pairs={{0,6},{1,7},{2,0},{3,1},{4,2},{5,3},{6,4},{7,5},{8,14},{9,15},{10,... | collective-permute-start | bytes 786440 | tf_op jit(solution)/shard_map/ppermute | solution.py:64
  135.0 2.0 collective-permute-start.8
  137.0 3.3 %collective-permute-start.7 = (bf16[64,2048]{1,0:T(8,128)(2,1)S(1)}, bf16[64,2048]{1,0:T(8,128)(2,1)S(1)}, u32[]{:S(2)}, u32[]{:S(2)}) collective-permute-start(bf16[64,2048]{1,0:T(8,128)(2,1)S(1)} %get-tuple-element.56), channel_id=1, source_target_pairs={{0,4},{1,5},{2,6},{3,7},{4,0},{5,1},{6,2},{7,3},{8,12},{9,13},{10,... | collective-permute-start | bytes 786440 | tf_op jit(solution)/shard_map/ppermute | solution.py:64
  140.3 10.7 %collective-permute-done.8 = bf16[64,2048]{1,0:T(8,128)(2,1)S(1)} collective-permute-done((bf16[64,2048]{1,0:T(8,128)(2,1)S(1)}, bf16[64,2048]{1,0:T(8,128)(2,1)S(1)}, u32[]{:S(2)}, u32[]{:S(2)}) %collective-permute-start.8) | collective-permute-done | bytes 262176 | tf_op jit(solution)/shard_map/ppermute | solution.py:64
  151.0 0.3 fusion.3
  151.3 0.1 fusion.5
  151.5 2.0 collective-permute-start.11
  153.4 2.5 %collective-permute-start.10 = (bf16[64,2048]{1,0:T(8,128)(2,1)S(1)}, bf16[64,2048]{1,0:T(8,128)(2,1)S(1)}, u32[]{:S(2)}, u32[]{:S(2)}) collective-permute-start(bf16[64,2048]{1,0:T(8,128)(2,1)S(1)} %fusion.5), channel_id=1, source_target_pairs={{0,4},{1,5},{2,6},{3,7},{4,0},{5,1},{6,2},{7,3},{8,12},{9,13},{10,... | collective-permute-start | bytes 786440 | tf_op jit(solution)/shard_map/ppermute | solution.py:64
  156.0 2.8 %collective-permute-start.9 = (bf16[64,2048]{1,0:T(8,128)(2,1)S(1)}, bf16[64,2048]{1,0:T(8,128)(2,1)S(1)}, u32[]{:S(2)}, u32[]{:S(2)}) collective-permute-start(bf16[64,2048]{1,0:T(8,128)(2,1)S(1)} %fusion.5), channel_id=1, source_target_pairs={{0,2},{1,3},{2,4},{3,5},{4,6},{5,7},{6,0},{7,1},{8,10},{9,11},{10,... | collective-permute-start | bytes 786440 | tf_op jit(solution)/shard_map/ppermute | solution.py:64
  158.8 1.0 collective-permute-done.11
  159.7 3.5 %collective-permute-done.10 = bf16[64,2048]{1,0:T(8,128)(2,1)S(1)} collective-permute-done((bf16[64,2048]{1,0:T(8,128)(2,1)S(1)}, bf16[64,2048]{1,0:T(8,128)(2,1)S(1)}, u32[]{:S(2)}, u32[]{:S(2)}) %collective-permute-start.10) | collective-permute-done | bytes 262176 | tf_op jit(solution)/shard_map/ppermute | solution.py:64
  163.2 7.2 %collective-permute-done.9 = bf16[64,2048]{1,0:T(8,128)(2,1)S(1)} collective-permute-done((bf16[64,2048]{1,0:T(8,128)(2,1)S(1)}, bf16[64,2048]{1,0:T(8,128)(2,1)S(1)}, u32[]{:S(2)}, u32[]{:S(2)}) %collective-permute-start.9) | collective-permute-done | bytes 262176 | tf_op jit(solution)/shard_map/ppermute | solution.py:64
  170.5 2.8 %collective-permute-start.12 = (bf16[256,2048]{1,0:T(8,128)(2,1)S(1)}, bf16[256,2048]{1,0:T(8,128)(2,1)S(1)}, u32[]{:S(2)}, u32[]{:S(2)}) collective-permute-start(bf16[256,2048]{1,0:T(8,128)(2,1)S(1)} %pad_maximum_fusion.own_ref), channel_id=1, source_target_pairs={{0,1},{1,0},{2,3},{3,2},{4,5},{5,4},{6,7},{7,6},{8,9},{9,8},{10,11... | collective-permute-start | bytes 3145736 | tf_op jit(solution)/shard_map/ppermute | solution.py:68
  173.3 2.3 collective-permute-done.12.other_ref
  175.5 4.8 %all-gather.2.cloned.1.call-done.up_ref.down_ref = bf16[2048,2048]{1,0:T(8,128)(2,1)} async-done(((bf16[64,2048]{1,0:T(8,128)(2,1)}), bf16[2048,2048]{1,0:T(8,128)(2,1)}) %all-gather.2.cloned.1.call-update) | async-done | bytes 8388624 | tf_op jit(solution)/shard_map/all_gather | solution.py:17
  180.4 3.4 %copy-done.1 = bf16[2048,2048]{1,0:T(8,128)(2,1)S(1)} copy-done((bf16[2048,2048]{1,0:T(8,128)(2,1)S(1)}, bf16[2048,2048]{1,0:T(8,128)(2,1)}, u32[]{:S(2)}) %copy-start.1) | copy-done | bytes 8388632
  183.7 6.4 %feed_forward.1 = bf16[512,2048]{1,0:T(8,128)(2,1)S(1)} custom-call(bf16[256,2048]{1,0:T(8,128)(2,1)S(1)} %pad_maximum_fusion.own_ref, bf16[256,2048]{1,0:T(8,128)(2,1)S(1)} %collective-permute-done.12.other_ref, bf16[2048,2048]{1,0:T(8,128)(2,1)S(1)} %copy-done.1, bf16[2048,2048]{1,0:T(8,128)(2,1)S(1)} %copy-done.1), custom_call_target="tpu_custom_call" | custom-call | flops 4294967296 | bytes 12582912 | tf_op jit(solution)/shard_map/feed_forward/pallas_call | solution.py:163
  190.2 19.2 %collective-permute-start.13 = (bf16[256,2048]{1,0:T(8,128)(2,1)S(1)}, bf16[256,2048]{1,0:T(8,128)(2,1)S(1)}, u32[]{:S(2)}, u32[]{:S(2)}) collective-permute-start(bf16[256,2048]{1,0:T(8,128)(2,1)S(1)} %slice.236), channel_id=1, source_target_pairs={{0,1},{1,0},{2,3},{3,2},{4,5},{5,4},{6,7},{7,6},{8,9},{9,8},{10,11... | collective-permute-start | bytes 3145736 | tf_op jit(solution)/shard_map/ppermute | solution.py:68
  209.5 2.3 collective-permute-done.13
  211.8 0.4 add_convert_fusion
  212.2 4.4 %collective-permute-start.14 = (bf16[64,2048]{1,0:T(8,128)(2,1)S(1)}, bf16[64,2048]{1,0:T(8,128)(2,1)S(1)}, u32[]{:S(2)}, u32[]{:S(2)}) collective-permute-start(bf16[64,2048]{1,0:T(8,128)(2,1)S(1)} %get-tuple-element.51), channel_id=1, source_target_pairs={{0,6},{1,7},{2,0},{3,1},{4,2},{5,3},{6,4},{7,5},{8,14},{9,15},{10,... | collective-permute-start | bytes 786440 | tf_op jit(solution)/shard_map/ppermute | solution.py:64
  216.6 2.0 collective-permute-start.16
  218.5 3.7 %collective-permute-start.15 = (bf16[64,2048]{1,0:T(8,128)(2,1)S(1)}, bf16[64,2048]{1,0:T(8,128)(2,1)S(1)}, u32[]{:S(2)}, u32[]{:S(2)}) collective-permute-start(bf16[64,2048]{1,0:T(8,128)(2,1)S(1)} %get-tuple-element.53), channel_id=1, source_target_pairs={{0,4},{1,5},{2,6},{3,7},{4,0},{5,1},{6,2},{7,3},{8,12},{9,13},{10,... | collective-permute-start | bytes 786440 | tf_op jit(solution)/shard_map/ppermute | solution.py:64
  222.2 5.6 %collective-permute-done.16 = bf16[64,2048]{1,0:T(8,128)(2,1)S(1)} collective-permute-done((bf16[64,2048]{1,0:T(8,128)(2,1)S(1)}, bf16[64,2048]{1,0:T(8,128)(2,1)S(1)}, u32[]{:S(2)}, u32[]{:S(2)}) %collective-permute-start.16) | collective-permute-done | bytes 262176 | tf_op jit(solution)/shard_map/ppermute | solution.py:64
  227.8 3.9 %collective-permute-done.15 = bf16[64,2048]{1,0:T(8,128)(2,1)S(1)} collective-permute-done((bf16[64,2048]{1,0:T(8,128)(2,1)S(1)}, bf16[64,2048]{1,0:T(8,128)(2,1)S(1)}, u32[]{:S(2)}, u32[]{:S(2)}) %collective-permute-start.15) | collective-permute-done | bytes 262176 | tf_op jit(solution)/shard_map/ppermute | solution.py:64
  231.7 0.9 fusion.6
  (93 shorter events, 1.9 us)
Async XLA Ops:
  6.5 113.8 %copy-start = (bf16[128,2048]{1,0:T(8,128)(2,1)S(1)}, bf16[128,2048]{1,0:T(8,128)(2,1)}, u32[]{:S(2)}) copy-start(bf16[128,2048]{1,0:T(8,128)(2,1)} %param.21) | copy-start | bytes 1572868
  6.6 173.8 %all-gather.2.cloned.1.call-start = ((), (), s32[]{:S(2)}) async-start(), calls=%async_computation | async-start | bytes 8650752 | tf_op jit(solution)/shard_map/all_gather | solution.py:17
  8.3 108.6 %copy-start.6 = (f32[1,512]{1,0:T(1,128)S(1)}, f32[1,512]{1,0:T(1,128)}, u32[]{:S(2)}) copy-start(f32[1,512]{1,0:T(1,128)} %param.17) | copy-start | bytes 6148
  25.4 93.2 %copy-start.3 = (bf16[512,128]{1,0:T(8,128)(2,1)S(1)}, bf16[512,128]{1,0:T(8,128)(2,1)}, u32[]{:S(2)}) copy-start(bf16[512,128]{1,0:T(8,128)(2,1)} %param.13) | copy-start | bytes 393220
  27.1 91.9 %copy-start.2 = (bf16[512,128]{1,0:T(8,128)(2,1)S(1)}, bf16[512,128]{1,0:T(8,128)(2,1)}, u32[]{:S(2)}) copy-start(bf16[512,128]{1,0:T(8,128)(2,1)} %param.15) | copy-start | bytes 393220
  28.6 6.3 %collective-permute-start = (bf16[1,144,128]{2,1,0:T(8,128)(2,1)S(1)}, bf16[1,144,128]{2,1,0:T(8,128)(2,1)S(1)}, u32[]{:S(2)}, u32[]{:S(2)}) collective-permute-start(bf16[1,144,128]{2,1,0:T(8,128)(2,1)S(1)} %fusion.28), channel_id=1, source_target_pairs={{0,8},{8,16},{16,24},{24,32},{32,40},{40,48},{48,56},{56,64},{64,7... | collective-permute-start | bytes 110600 | tf_op jit(solution)/shard_map/ppermute | solution.py:22
  37.5 7.7 %collective-permute-start.1 = (bf16[1,144,128]{2,1,0:T(8,128)(2,1)S(1)}, bf16[1,144,128]{2,1,0:T(8,128)(2,1)S(1)}, u32[]{:S(2)}, u32[]{:S(2)}) collective-permute-start(bf16[1,144,128]{2,1,0:T(8,128)(2,1)S(1)} %fusion.29), channel_id=1, source_target_pairs={{0,16},{8,24},{16,32},{24,40},{32,48},{40,56},{48,64},{56,72},{64,... | collective-permute-start | bytes 110600 | tf_op jit(solution)/shard_map/ppermute | solution.py:22
  45.3 74.6 %copy-start.5 = (bf16[512,128]{1,0:T(8,128)(2,1)S(1)}, bf16[512,128]{1,0:T(8,128)(2,1)}, u32[]{:S(2)}) copy-start(bf16[512,128]{1,0:T(8,128)(2,1)} %param.16) | copy-start | bytes 393220
  45.3 74.6 %copy-start.8 = (f32[128]{0:T(128)S(1)}, f32[128]{0:T(128)}, u32[]{:S(2)}) copy-start(f32[128]{0:T(128)} %param.20) | copy-start | bytes 1540
  45.4 13.6 %collective-permute-start.2 = (bf16[1,144,128]{2,1,0:T(8,128)(2,1)S(1)}, bf16[1,144,128]{2,1,0:T(8,128)(2,1)S(1)}, u32[]{:S(2)}, u32[]{:S(2)}) collective-permute-start(bf16[1,144,128]{2,1,0:T(8,128)(2,1)S(1)} %fusion.30), channel_id=1, source_target_pairs={{0,32},{8,40},{16,48},{24,56},{32,64},{40,72},{48,80},{56,88},{64,... | collective-permute-start | bytes 110600 | tf_op jit(solution)/shard_map/ppermute | solution.py:22
  59.1 24.0 %collective-permute-start.3 = (bf16[1,144,128]{2,1,0:T(8,128)(2,1)S(1)}, bf16[1,144,128]{2,1,0:T(8,128)(2,1)S(1)}, u32[]{:S(2)}, u32[]{:S(2)}) collective-permute-start(bf16[1,144,128]{2,1,0:T(8,128)(2,1)S(1)} %fusion.31), channel_id=1, source_target_pairs={{0,64},{8,72},{16,80},{24,88},{32,96},{40,104},{48,112},{56,120},{... | collective-permute-start | bytes 110600 | tf_op jit(solution)/shard_map/ppermute | solution.py:22
  83.3 34.8 %collective-permute-start.4 = (bf16[1,144,128]{2,1,0:T(8,128)(2,1)S(1)}, bf16[1,144,128]{2,1,0:T(8,128)(2,1)S(1)}, u32[]{:S(2)}, u32[]{:S(2)}) collective-permute-start(bf16[1,144,128]{2,1,0:T(8,128)(2,1)S(1)} %fusion.32), channel_id=1, source_target_pairs={{0,128},{8,136},{16,144},{24,152},{32,160},{40,168},{48,176},{56,1... | collective-permute-start | bytes 110600 | tf_op jit(solution)/shard_map/ppermute | solution.py:22
  121.1 29.9 %copy-start.4 = (bf16[64,2048]{1,0:T(8,128)(2,1)S(1)}, bf16[64,2048]{1,0:T(8,128)(2,1)}, u32[]{:S(2)}) copy-start(bf16[64,2048]{1,0:T(8,128)(2,1)} %param.22) | copy-start | bytes 786436
  121.1 8.8 %collective-permute-start.5 = (bf16[256,2048]{1,0:T(8,128)(2,1)S(1)}, bf16[256,2048]{1,0:T(8,128)(2,1)S(1)}, u32[]{:S(2)}, u32[]{:S(2)}) collective-permute-start(bf16[256,2048]{1,0:T(8,128)(2,1)S(1)} %slice.230), channel_id=1, source_target_pairs={{0,1},{1,0},{2,3},{3,2},{4,5},{5,4},{6,7},{7,6},{8,9},{9,8},{10,11... | collective-permute-start | bytes 3145736 | tf_op jit(solution)/shard_map/ppermute | solution.py:68
  130.3 21.0 %copy-start.7 = (f32[2048]{0:T(1024)S(1)}, f32[2048]{0:T(1024)}, u32[]{:S(2)}) copy-start(f32[2048]{0:T(1024)} %param.23) | copy-start | bytes 24580
  130.4 9.9 %collective-permute-start.6 = (bf16[64,2048]{1,0:T(8,128)(2,1)S(1)}, bf16[64,2048]{1,0:T(8,128)(2,1)S(1)}, u32[]{:S(2)}, u32[]{:S(2)}) collective-permute-start(bf16[64,2048]{1,0:T(8,128)(2,1)S(1)} %get-tuple-element.54), channel_id=1, source_target_pairs={{0,6},{1,7},{2,0},{3,1},{4,2},{5,3},{6,4},{7,5},{8,14},{9,15},{10,... | collective-permute-start | bytes 786440 | tf_op jit(solution)/shard_map/ppermute | solution.py:64
  135.0 16.0 %collective-permute-start.8 = (bf16[64,2048]{1,0:T(8,128)(2,1)S(1)}, bf16[64,2048]{1,0:T(8,128)(2,1)S(1)}, u32[]{:S(2)}, u32[]{:S(2)}) collective-permute-start(bf16[64,2048]{1,0:T(8,128)(2,1)S(1)} %get-tuple-element.55), channel_id=1, source_target_pairs={{0,2},{1,3},{2,4},{3,5},{4,6},{5,7},{6,0},{7,1},{8,10},{9,11},{10,... | collective-permute-start | bytes 786440 | tf_op jit(solution)/shard_map/ppermute | solution.py:64
  137.0 14.0 %collective-permute-start.7 = (bf16[64,2048]{1,0:T(8,128)(2,1)S(1)}, bf16[64,2048]{1,0:T(8,128)(2,1)S(1)}, u32[]{:S(2)}, u32[]{:S(2)}) collective-permute-start(bf16[64,2048]{1,0:T(8,128)(2,1)S(1)} %get-tuple-element.56), channel_id=1, source_target_pairs={{0,4},{1,5},{2,6},{3,7},{4,0},{5,1},{6,2},{7,3},{8,12},{9,13},{10,... | collective-permute-start | bytes 786440 | tf_op jit(solution)/shard_map/ppermute | solution.py:64
  151.5 8.3 %collective-permute-start.11 = (bf16[64,2048]{1,0:T(8,128)(2,1)S(1)}, bf16[64,2048]{1,0:T(8,128)(2,1)S(1)}, u32[]{:S(2)}, u32[]{:S(2)}) collective-permute-start(bf16[64,2048]{1,0:T(8,128)(2,1)S(1)} %fusion.5), channel_id=1, source_target_pairs={{0,6},{1,7},{2,0},{3,1},{4,2},{5,3},{6,4},{7,5},{8,14},{9,15},{10,... | collective-permute-start | bytes 786440 | tf_op jit(solution)/shard_map/ppermute | solution.py:64
  153.4 9.8 %collective-permute-start.10 = (bf16[64,2048]{1,0:T(8,128)(2,1)S(1)}, bf16[64,2048]{1,0:T(8,128)(2,1)S(1)}, u32[]{:S(2)}, u32[]{:S(2)}) collective-permute-start(bf16[64,2048]{1,0:T(8,128)(2,1)S(1)} %fusion.5), channel_id=1, source_target_pairs={{0,4},{1,5},{2,6},{3,7},{4,0},{5,1},{6,2},{7,3},{8,12},{9,13},{10,... | collective-permute-start | bytes 786440 | tf_op jit(solution)/shard_map/ppermute | solution.py:64
  156.0 14.4 %collective-permute-start.9 = (bf16[64,2048]{1,0:T(8,128)(2,1)S(1)}, bf16[64,2048]{1,0:T(8,128)(2,1)S(1)}, u32[]{:S(2)}, u32[]{:S(2)}) collective-permute-start(bf16[64,2048]{1,0:T(8,128)(2,1)S(1)} %fusion.5), channel_id=1, source_target_pairs={{0,2},{1,3},{2,4},{3,5},{4,6},{5,7},{6,0},{7,1},{8,10},{9,11},{10,... | collective-permute-start | bytes 786440 | tf_op jit(solution)/shard_map/ppermute | solution.py:64
  170.5 5.0 %collective-permute-start.12 = (bf16[256,2048]{1,0:T(8,128)(2,1)S(1)}, bf16[256,2048]{1,0:T(8,128)(2,1)S(1)}, u32[]{:S(2)}, u32[]{:S(2)}) collective-permute-start(bf16[256,2048]{1,0:T(8,128)(2,1)S(1)} %pad_maximum_fusion.own_ref), channel_id=1, source_target_pairs={{0,1},{1,0},{2,3},{3,2},{4,5},{5,4},{6,7},{7,6},{8,9},{9,8},{10,11... | collective-permute-start | bytes 3145736 | tf_op jit(solution)/shard_map/ppermute | solution.py:68
  180.4 3.4 %copy-start.1 = (bf16[2048,2048]{1,0:T(8,128)(2,1)S(1)}, bf16[2048,2048]{1,0:T(8,128)(2,1)}, u32[]{:S(2)}) copy-start(bf16[2048,2048]{1,0:T(8,128)(2,1)} %all-gather.2.cloned.1.call-done.up_ref.down_ref) | copy-start | bytes 25165828
  190.2 21.5 %collective-permute-start.13 = (bf16[256,2048]{1,0:T(8,128)(2,1)S(1)}, bf16[256,2048]{1,0:T(8,128)(2,1)S(1)}, u32[]{:S(2)}, u32[]{:S(2)}) collective-permute-start(bf16[256,2048]{1,0:T(8,128)(2,1)S(1)} %slice.236), channel_id=1, source_target_pairs={{0,1},{1,0},{2,3},{3,2},{4,5},{5,4},{6,7},{7,6},{8,9},{9,8},{10,11... | collective-permute-start | bytes 3145736 | tf_op jit(solution)/shard_map/ppermute | solution.py:68
  212.2 10.0 %collective-permute-start.14 = (bf16[64,2048]{1,0:T(8,128)(2,1)S(1)}, bf16[64,2048]{1,0:T(8,128)(2,1)S(1)}, u32[]{:S(2)}, u32[]{:S(2)}) collective-permute-start(bf16[64,2048]{1,0:T(8,128)(2,1)S(1)} %get-tuple-element.51), channel_id=1, source_target_pairs={{0,6},{1,7},{2,0},{3,1},{4,2},{5,3},{6,4},{7,5},{8,14},{9,15},{10,... | collective-permute-start | bytes 786440 | tf_op jit(solution)/shard_map/ppermute | solution.py:64
  216.6 11.2 %collective-permute-start.16 = (bf16[64,2048]{1,0:T(8,128)(2,1)S(1)}, bf16[64,2048]{1,0:T(8,128)(2,1)S(1)}, u32[]{:S(2)}, u32[]{:S(2)}) collective-permute-start(bf16[64,2048]{1,0:T(8,128)(2,1)S(1)} %get-tuple-element.52), channel_id=1, source_target_pairs={{0,2},{1,3},{2,4},{3,5},{4,6},{5,7},{6,0},{7,1},{8,10},{9,11},{10,... | collective-permute-start | bytes 786440 | tf_op jit(solution)/shard_map/ppermute | solution.py:64
  218.5 13.1 %collective-permute-start.15 = (bf16[64,2048]{1,0:T(8,128)(2,1)S(1)}, bf16[64,2048]{1,0:T(8,128)(2,1)S(1)}, u32[]{:S(2)}, u32[]{:S(2)}) collective-permute-start(bf16[64,2048]{1,0:T(8,128)(2,1)S(1)} %get-tuple-element.53), channel_id=1, source_target_pairs={{0,4},{1,5},{2,6},{3,7},{4,0},{5,1},{6,2},{7,3},{8,12},{9,13},{10,... | collective-permute-start | bytes 786440 | tf_op jit(solution)/shard_map/ppermute | solution.py:64
Sparse Core Ops, SparseCore 0:
  9.4 170.8 all-gather.1

commit v3 on v2

--- a/solution.py
+++ b/solution.py
@@ -59,43 +59,37 @@
     return earlier
 
 
-def turned_by(x, axis, steps):
-    length = lax.axis_size(axis)
-    return lax.ppermute(x, axis, [(k, (k + steps) % length) for k in range(length)])
-
-
 def with_partner(x, axis):
     return lax.ppermute(x, axis, [(k, k ^ 1) for k in range(lax.axis_size(axis))])
 
 
-def in_relative_order(x, axis):
+def among_chips(blocks, axis):
+    length = lax.axis_size(axis)
+    groups = [list(range(core, length, 2)) for core in range(2)]
+    return lax.all_to_all(blocks, axis, 0, 0, tiled=True, axis_index_groups=groups)
+
+
+def own_core_first(x, axis):
     chips = lax.axis_size(axis) // 2
-    place = lax.axis_index(axis)
-    chip, core = (place // 2, place % 2)
+    core = lax.axis_index(axis) % 2
     blocks = x.reshape(chips, 2, -1, x.shape[-1])
-    blocks = jnp.where(core == 0, blocks, blocks[:, ::-1])
-    rows = [
-        lax.dynamic_index_in_dim(blocks, (chip - d + chips) % chips, 0, False) for d in range(chips)
-    ]
-    return jnp.concatenate([r[0] for r in rows] + [r[1] for r in rows], axis=0)
-
-
-def sum_of_relative_rows(kept, sent, axis):
+    first = jnp.where(core == 0, blocks[:, 0], blocks[:, 1])
+    second = jnp.where(core == 0, blocks[:, 1], blocks[:, 0])
+    return jnp.concatenate([first, second], axis=0).reshape(x.shape)
+
+
+def sum_at_owner(rows, axis):
     chips = lax.axis_size(axis) // 2
-    found = with_partner(sent, axis)
-    both = (kept.astype(jnp.float32) + found.astype(jnp.float32)).astype(jnp.bfloat16)
-    blocks = both.reshape(chips, -1, both.shape[-1])
-    arrived = {d: turned_by(blocks[d], axis, -2 * d) for d in (2, 1, 3)}
-    total = blocks[0].astype(jnp.float32)
-    for d in range(1, chips):
-        total = total + arrived[d].astype(jnp.float32)
-    return total
-
-
-def relative_rows(x, axis):
+    half = rows.shape[0] // 2
+    found = with_partner(rows[half:], axis)
+    both = (rows[:half].astype(jnp.float32) + found.astype(jnp.float32)).astype(jnp.bfloat16)
+    blocks = among_chips(both.reshape(chips, -1, both.shape[-1]), axis)
+    return jnp.sum(blocks.astype(jnp.float32), axis=0)
+
+
+def rows_of_all(x, axis):
     chips = lax.axis_size(axis) // 2
-    found = {d: turned_by(x, axis, 2 * d) for d in (2, 1, 3)}
-    own = jnp.concatenate([x] + [found[d] for d in range(1, chips)], axis=0)
+    own = among_chips(jnp.broadcast_to(x, (chips, *x.shape)), axis).reshape(-1, x.shape[-1])
     return own, with_partner(own, axis)
 
 
@@ -129,7 +123,7 @@
     memory = jnp.sum(scale[..., None, None] * memories[None], axis=1)
     lanes = (count + 1, totals.shape[1], 1, memories.shape[-1])
     spread = lambda x: jnp.broadcast_to(x[..., None, None], lanes)
-    return spread(total), spread(top), memory
+    return (*lax.optimization_barrier((spread(total), spread(top))), memory)
 
 
 def feed_forward_kernel(own_ref, other_ref, up_ref, down_ref, out_ref, active_ref):
@@ -173,7 +167,7 @@
         out_specs=pl.BlockSpec((2 * half, down_height), lambda i: (0, jnp.maximum(i - ups, 0))),
         scratch_shapes=[pltpu.VMEM((2 * half, hidden), jnp.bfloat16)],
         compiler_params=pltpu.CompilerParams(
-            dimension_semantics=("arbitrary",), vmem_limit_bytes=40 * 1024 * 1024
+            dimension_semantics=("arbitrary",), vmem_limit_bytes=48 * 1024 * 1024
         ),
         cost_estimate=pl.CostEstimate(
             flops=8 * half * features * hidden,
@@ -267,17 +261,16 @@
         output_preactivation.astype(jnp.float32).reshape(tok_count, head_count, head_dim)
     )
     mixed = gated.reshape(tok_count, head_count * head_dim).astype(jnp.bfloat16)
-    mixed = in_relative_order(mixed, "tp")
+    mixed = own_core_first(mixed, "tp")
     partial_branch = jnp.dot(
         mixed, output_projection_matrix, preferred_element_type=jnp.float32
     ).astype(jnp.bfloat16)
-    middle = tok_count // 2
-    branch = sum_of_relative_rows(partial_branch[:middle], partial_branch[middle:], "tp")
+    branch = sum_at_owner(partial_branch, "tp")
     mid_state = (residual.astype(jnp.float32) + branch).astype(jnp.bfloat16)
     normed = rms_norm(mid_state.astype(jnp.float32), feedforward_norm_gain).astype(jnp.bfloat16)
-    own, other = relative_rows(normed, "tp")
+    own, other = rows_of_all(normed, "tp")
     mlp_rows = feed_forward(own, other, weights, feedforward_up_matrix.shape[1])
-    mlp_sum = sum_of_relative_rows(mlp_rows[:middle], mlp_rows[middle:], "tp")
+    mlp_sum = sum_at_owner(mlp_rows, "tp")
     return (mid_state.astype(jnp.float32) + mlp_sum).astype(jnp.bfloat16)
 
 

time: 241 us -> 236 us (0.979)
  blocking collectives: 0 us -> 53 us
  starting transfers between devices: 136 us -> 109 us
  waiting for transfers between devices: 48.5 us -> 36.1 us
  between operations: 25 us -> 14 us
  local copies, waits for them, and re-layouts: 6.95 us -> 1.21 us
    all_to_all x0 -> x3, blocking collectives: none -> 53 us  [among_chips(): lax.all_to_all(blocks, axis, 0, 0, tiled=True, axis_index_groups=groups)]
    ppermute x9 -> x0, waiting for transfers between devices: 31.7 us -> none  [turned_by(): lax.ppermute(x, axis, [(k, (k + steps) % length) for k in range(length)])]
    ppermute x9 -> x0, starting transfers between devices: 27.2 us -> none  [turned_by(): lax.ppermute(x, axis, [(k, (k + steps) % length) for k in range(length)])]
    all_gather x1, waiting for transfers between devices: 4.84 us -> 24.1 us  [gathered_weights(): lax.all_gather(jnp.concatenate([up, down.T], axis=1), axis, axis=0, tiled...]
    unnamed x25 -> x16, local copies, waits for them, and re-layouts: 3.54 us -> 0.05 us
  transfers between devices with their start and end apart: 18 -> 9, of which waited for: 15 -> 9; matrix products, arithmetic and copies ran while one was open for 7% -> 5% of each run, Pallas kernels for 0% -> 0%
where the time goes in v3:
time: 236 us
  starting transfers between devices  109 us (46%)
  blocking collectives  53 us (22%)
  waiting for transfers between devices  36.1 us (15%)
  between operations  14 us (6%)
  other arithmetic  10.1 us (4%)
  Pallas kernels  8.52 us (4%)
  matrix products  3.6 us (2%)
    ppermute x5, starting transfers between devices, shifted_on(): lax.ppermute(x, axis, [(k, k + distance) for k in range(length - distance)])  78.7 us
    all_to_all x3, blocking collectives, among_chips(): lax.all_to_all(blocks, axis, 0, 0, tiled=True, axis_index_groups=groups)  53 us
    ppermute x3, starting transfers between devices, with_partner(): lax.ppermute(x, axis, [(k, k ^ 1) for k in range(lax.axis_size(axis))])  30.3 us
    all_gather x1, waiting for transfers between devices, gathered_weights(): lax.all_gather(jnp.concatenate([up, down.T], axis=1), axis, axis=0, tiled...  24.1 us
    pallas_call x1, Pallas kernels, feed_forward(): pl.pallas_call(feed_forward_kernel, grid=(ups + downs,), out_shape=jax.Sh...  8.52 us
    ppermute x3, waiting for transfers between devices, with_partner(): lax.ppermute(x, axis, [(k, k ^ 1) for k in range(lax.axis_size(axis))])  6.79 us
    ppermute x5, waiting for transfers between devices, shifted_on(): lax.ppermute(x, axis, [(k, k + distance) for k in range(length - distance)])  5.12 us
  transfers between devices with their start and end apart: 9, of which 9 were waited for; matrix products, arithmetic and copies ran while one was open for 5% of the time, Pallas kernels for 0%

profile of v3, /device:TPU:33, one launch (start us, length us, event | category | flops | bytes accessed | tf_op | source)
XLA Modules:
  0.0 235.5 jit_solution(4475114480691150045)
XLA Ops:
  6.6 1.7 pad_maximum_fusion
  8.3 0.1 all-gather.2.cloned.1.call-update
  8.4 0.7 fusion.45
  9.1 1.2 reduce_window_sum.11
  10.3 0.2 slice_reduce_fusion.12
  10.5 0.1 fusion.43
  10.6 0.1 select_reduce_fusion.1
  10.7 0.9 fusion.44
  11.5 0.1 fusion.46
  11.6 0.1 fusion.42
  11.7 0.1 copy.34
  11.8 0.9 convert_multiply_fusion.2
  12.8 0.8 subtract_exponential_fusion.1
  13.5 1.6 fusion.13
  15.1 0.0 copy-start.2
  15.1 0.2 multiply_reduce_fusion
  15.3 0.0 copy-start.1
  15.3 0.2 slice_reduce_fusion
  15.6 5.2 %collective-permute-start = (bf16[1,144,128]{2,1,0:T(8,128)(2,1)S(1)}, bf16[1,144,128]{2,1,0:T(8,128)(2,1)S(1)}, u32[]{:S(2)}, u32[]{:S(2)}) collective-permute-start(bf16[1,144,128]{2,1,0:T(8,128)(2,1)S(1)} %fusion.30), channel_id=1, source_target_pairs={{0,8},{8,16},{16,24},{24,32},{32,40},{40,48},{48,56},{56,64},{64,7... | collective-permute-start | bytes 110600 | tf_op jit(solution)/shard_map/ppermute | solution.py:22
  20.8 1.0 collective-permute-done
  22.0 6.6 %collective-permute-start.1 = (bf16[1,144,128]{2,1,0:T(8,128)(2,1)S(1)}, bf16[1,144,128]{2,1,0:T(8,128)(2,1)S(1)}, u32[]{:S(2)}, u32[]{:S(2)}) collective-permute-start(bf16[1,144,128]{2,1,0:T(8,128)(2,1)S(1)} %fusion.31), channel_id=1, source_target_pairs={{0,16},{8,24},{16,32},{24,40},{32,48},{40,56},{48,64},{56,72},{64,... | collective-permute-start | bytes 110600 | tf_op jit(solution)/shard_map/ppermute | solution.py:22
  28.7 1.0 collective-permute-done.1
  29.9 12.4 %collective-permute-start.2 = (bf16[1,144,128]{2,1,0:T(8,128)(2,1)S(1)}, bf16[1,144,128]{2,1,0:T(8,128)(2,1)S(1)}, u32[]{:S(2)}, u32[]{:S(2)}) collective-permute-start(bf16[1,144,128]{2,1,0:T(8,128)(2,1)S(1)} %fusion.32), channel_id=1, source_target_pairs={{0,32},{8,40},{16,48},{24,56},{32,64},{40,72},{48,80},{56,88},{64,... | collective-permute-start | bytes 110600 | tf_op jit(solution)/shard_map/ppermute | solution.py:22
  42.3 1.0 collective-permute-done.2
  43.5 0.0 copy-start.4
  43.5 0.0 copy-start.7
  43.6 22.9 %collective-permute-start.3 = (bf16[1,144,128]{2,1,0:T(8,128)(2,1)S(1)}, bf16[1,144,128]{2,1,0:T(8,128)(2,1)S(1)}, u32[]{:S(2)}, u32[]{:S(2)}) collective-permute-start(bf16[1,144,128]{2,1,0:T(8,128)(2,1)S(1)} %fusion.33), channel_id=1, source_target_pairs={{0,64},{8,72},{16,80},{24,88},{32,96},{40,104},{48,112},{56,120},{... | collective-permute-start | bytes 110600 | tf_op jit(solution)/shard_map/ppermute | solution.py:22
  66.5 0.1 copy.33
  66.6 0.9 collective-permute-done.3
  67.6 31.5 %collective-permute-start.4 = (bf16[1,144,128]{2,1,0:T(8,128)(2,1)S(1)}, bf16[1,144,128]{2,1,0:T(8,128)(2,1)S(1)}, u32[]{:S(2)}, u32[]{:S(2)}) collective-permute-start(bf16[1,144,128]{2,1,0:T(8,128)(2,1)S(1)} %fusion.34), channel_id=1, source_target_pairs={{0,128},{8,136},{16,144},{24,152},{32,160},{40,168},{48,176},{56,1... | collective-permute-start | bytes 110600 | tf_op jit(solution)/shard_map/ppermute | solution.py:22
  99.2 0.2 select_reduce_fusion
  99.4 1.1 collective-permute-done.4
  100.6 0.1 exponential_bitcast_fusion.1
  100.7 0.1 copy.37
  100.8 0.1 copy.38
  100.9 0.1 subtract_exponential_fusion
  101.1 0.4 fusion.2
  101.5 0.4 fusion.93
  101.9 0.5 multiply_reduce_fusion.1
  102.4 0.1 fusion.11
  102.6 0.7 convolution_convert_fusion
  103.3 0.1 slice.151
  103.4 6.8 %collective-permute-start.5 = (bf16[256,2048]{1,0:T(8,128)(2,1)S(1)}, bf16[256,2048]{1,0:T(8,128)(2,1)S(1)}, u32[]{:S(2)}, u32[]{:S(2)}) collective-permute-start(bf16[256,2048]{1,0:T(8,128)(2,1)S(1)} %slice.151), channel_id=1, source_target_pairs={{0,1},{1,0},{2,3},{3,2},{4,5},{5,4},{6,7},{7,6},{8,9},{9,8},{10,11... | collective-permute-start | bytes 3145736 | tf_op jit(solution)/shard_map/ppermute | solution.py:63
  110.2 2.3 collective-permute-done.5
  112.5 0.4 add_convert_fusion.1
  112.9 0.0 copy-start.3
  112.9 0.0 copy-start.6
  112.9 18.9 %all_to_all.15 = bf16[4,64,2048]{2,1,0:T(8,128)(2,1)S(1)} all-to-all(bf16[4,64,2048]{2,1,0:T(8,128)(2,1)S(1)} %bitcast.138), channel_id=1, replica_groups={{0,2,4,6},{1,3,5,7},{8,10,12,14},{9,11,13,15},{16,18,20,22},{17,19,21,2..., dimensions={0} | all-to-all | bytes 2097152 | tf_op jit(solution)/shard_map/all_to_all | solution.py:69
  131.8 0.2 convert_reduce_fusion.1
  132.0 0.2 fusion.3
  132.2 0.1 fusion.5
  132.3 0.1 broadcast_in_dim.106
  132.4 15.9 %all_to_all.16 = bf16[4,64,2048]{2,1,0:T(8,128)(2,1)S(1)} all-to-all(bf16[4,64,2048]{2,1,0:T(8,128)(2,1)S(1)} %broadcast_in_dim.106), channel_id=1, replica_groups={{0,2,4,6},{1,3,5,7},{8,10,12,14},{9,11,13,15},{16,18,20,22},{17,19,21,2..., dimensions={0} | all-to-all | bytes 2097152 | tf_op jit(solution)/shard_map/all_to_all | solution.py:69
  148.3 4.5 %collective-permute-start.6 = (bf16[256,2048]{1,0:T(8,128)(2,1)S(1)}, bf16[256,2048]{1,0:T(8,128)(2,1)S(1)}, u32[]{:S(2)}, u32[]{:S(2)}) collective-permute-start(bf16[256,2048]{1,0:T(8,128)(2,1)S(1)} %bitcast.136), channel_id=1, source_target_pairs={{0,1},{1,0},{2,3},{3,2},{4,5},{5,4},{6,7},{7,6},{8,9},{9,8},{10,11... | collective-permute-start | bytes 3145736 | tf_op jit(solution)/shard_map/ppermute | solution.py:63
  152.9 2.3 collective-permute-done.6.other_ref
  155.1 24.1 %all-gather.2.cloned.1.call-done.up_ref.down_ref = bf16[2048,2048]{1,0:T(8,128)(2,1)} async-done(((bf16[64,2048]{1,0:T(8,128)(2,1)}), bf16[2048,2048]{1,0:T(8,128)(2,1)}) %all-gather.2.cloned.1.call-update) | async-done | bytes 8388624 | tf_op jit(solution)/shard_map/all_gather | solution.py:17
  179.3 8.5 %feed_forward.1 = bf16[512,2048]{1,0:T(8,128)(2,1)S(1)} custom-call(bf16[256,2048]{1,0:T(8,128)(2,1)S(1)} %bitcast.137, bf16[256,2048]{1,0:T(8,128)(2,1)S(1)} %collective-permute-done.6.other_ref, bf16[2048,2048]{1,0:T(8,128)(2,1)} %all-gather.2.cloned.1.call-done.up_ref.down_ref, bf16[2048,2048]{1,0:T(8,128)(2,1)} %all-gather.2.cloned.1.call-done.up_ref.down_ref), custom_call_target="tpu_custom_call" | custom-call | flops 4294967296 | bytes 12582912 | tf_op jit(solution)/shard_map/feed_forward/pallas_call | solution.py:157
  187.8 0.1 slice.153
  187.9 19.0 %collective-permute-start.7 = (bf16[256,2048]{1,0:T(8,128)(2,1)S(1)}, bf16[256,2048]{1,0:T(8,128)(2,1)S(1)}, u32[]{:S(2)}, u32[]{:S(2)}) collective-permute-start(bf16[256,2048]{1,0:T(8,128)(2,1)S(1)} %slice.153), channel_id=1, source_target_pairs={{0,1},{1,0},{2,3},{3,2},{4,5},{5,4},{6,7},{7,6},{8,9},{9,8},{10,11... | collective-permute-start | bytes 3145736 | tf_op jit(solution)/shard_map/ppermute | solution.py:63
  206.9 2.3 collective-permute-done.7
  209.1 0.4 add_convert_fusion
  209.5 18.2 %all_to_all.17 = bf16[4,64,2048]{2,1,0:T(8,128)(2,1)S(1)} all-to-all(bf16[4,64,2048]{2,1,0:T(8,128)(2,1)S(1)} %bitcast.139), channel_id=1, replica_groups={{0,2,4,6},{1,3,5,7},{8,10,12,14},{9,11,13,15},{16,18,20,22},{17,19,21,2..., dimensions={0} | all-to-all | bytes 2097152 | tf_op jit(solution)/shard_map/all_to_all | solution.py:69
  227.8 0.2 convert_reduce_fusion
  227.9 0.8 fusion.6
  (71 shorter events, 0.9 us)
Async XLA Ops:
  6.5 96.1 %copy-start = (bf16[128,2048]{1,0:T(8,128)(2,1)S(1)}, bf16[128,2048]{1,0:T(8,128)(2,1)}, u32[]{:S(2)}) copy-start(bf16[128,2048]{1,0:T(8,128)(2,1)} %param.21) | copy-start | bytes 1572868
  6.6 172.7 %all-gather.2.cloned.1.call-start = ((), (), s32[]{:S(2)}) async-start(), calls=%async_computation.3 | async-start | bytes 8650752 | tf_op jit(solution)/shard_map/all_gather | solution.py:17
  8.3 90.9 %copy-start.5 = (f32[1,512]{1,0:T(1,128)S(1)}, f32[1,512]{1,0:T(1,128)}, u32[]{:S(2)}) copy-start(f32[1,512]{1,0:T(1,128)} %param.17) | copy-start | bytes 6148
  15.1 85.9 %copy-start.2 = (bf16[512,128]{1,0:T(8,128)(2,1)S(1)}, bf16[512,128]{1,0:T(8,128)(2,1)}, u32[]{:S(2)}) copy-start(bf16[512,128]{1,0:T(8,128)(2,1)} %param.13) | copy-start | bytes 393220
  15.3 86.2 %copy-start.1 = (bf16[512,128]{1,0:T(8,128)(2,1)S(1)}, bf16[512,128]{1,0:T(8,128)(2,1)}, u32[]{:S(2)}) copy-start(bf16[512,128]{1,0:T(8,128)(2,1)} %param.15) | copy-start | bytes 393220
  15.6 6.3 %collective-permute-start = (bf16[1,144,128]{2,1,0:T(8,128)(2,1)S(1)}, bf16[1,144,128]{2,1,0:T(8,128)(2,1)S(1)}, u32[]{:S(2)}, u32[]{:S(2)}) collective-permute-start(bf16[1,144,128]{2,1,0:T(8,128)(2,1)S(1)} %fusion.30), channel_id=1, source_target_pairs={{0,8},{8,16},{16,24},{24,32},{32,40},{40,48},{48,56},{56,64},{64,7... | collective-permute-start | bytes 110600 | tf_op jit(solution)/shard_map/ppermute | solution.py:22
  22.0 7.7 %collective-permute-start.1 = (bf16[1,144,128]{2,1,0:T(8,128)(2,1)S(1)}, bf16[1,144,128]{2,1,0:T(8,128)(2,1)S(1)}, u32[]{:S(2)}, u32[]{:S(2)}) collective-permute-start(bf16[1,144,128]{2,1,0:T(8,128)(2,1)S(1)} %fusion.31), channel_id=1, source_target_pairs={{0,16},{8,24},{16,32},{24,40},{32,48},{40,56},{48,64},{56,72},{64,... | collective-permute-start | bytes 110600 | tf_op jit(solution)/shard_map/ppermute | solution.py:22
  29.9 13.5 %collective-permute-start.2 = (bf16[1,144,128]{2,1,0:T(8,128)(2,1)S(1)}, bf16[1,144,128]{2,1,0:T(8,128)(2,1)S(1)}, u32[]{:S(2)}, u32[]{:S(2)}) collective-permute-start(bf16[1,144,128]{2,1,0:T(8,128)(2,1)S(1)} %fusion.32), channel_id=1, source_target_pairs={{0,32},{8,40},{16,48},{24,56},{32,64},{40,72},{48,80},{56,88},{64,... | collective-permute-start | bytes 110600 | tf_op jit(solution)/shard_map/ppermute | solution.py:22
  43.5 58.9 %copy-start.4 = (bf16[512,128]{1,0:T(8,128)(2,1)S(1)}, bf16[512,128]{1,0:T(8,128)(2,1)}, u32[]{:S(2)}) copy-start(bf16[512,128]{1,0:T(8,128)(2,1)} %param.16) | copy-start | bytes 393220
  43.5 58.9 %copy-start.7 = (f32[128]{0:T(128)S(1)}, f32[128]{0:T(128)}, u32[]{:S(2)}) copy-start(f32[128]{0:T(128)} %param.20) | copy-start | bytes 1540
  43.6 23.9 %collective-permute-start.3 = (bf16[1,144,128]{2,1,0:T(8,128)(2,1)S(1)}, bf16[1,144,128]{2,1,0:T(8,128)(2,1)S(1)}, u32[]{:S(2)}, u32[]{:S(2)}) collective-permute-start(bf16[1,144,128]{2,1,0:T(8,128)(2,1)S(1)} %fusion.33), channel_id=1, source_target_pairs={{0,64},{8,72},{16,80},{24,88},{32,96},{40,104},{48,112},{56,120},{... | collective-permute-start | bytes 110600 | tf_op jit(solution)/shard_map/ppermute | solution.py:22
  67.6 32.9 %collective-permute-start.4 = (bf16[1,144,128]{2,1,0:T(8,128)(2,1)S(1)}, bf16[1,144,128]{2,1,0:T(8,128)(2,1)S(1)}, u32[]{:S(2)}, u32[]{:S(2)}) collective-permute-start(bf16[1,144,128]{2,1,0:T(8,128)(2,1)S(1)} %fusion.34), channel_id=1, source_target_pairs={{0,128},{8,136},{16,144},{24,152},{32,160},{40,168},{48,176},{56,1... | collective-permute-start | bytes 110600 | tf_op jit(solution)/shard_map/ppermute | solution.py:22
  103.4 9.1 %collective-permute-start.5 = (bf16[256,2048]{1,0:T(8,128)(2,1)S(1)}, bf16[256,2048]{1,0:T(8,128)(2,1)S(1)}, u32[]{:S(2)}, u32[]{:S(2)}) collective-permute-start(bf16[256,2048]{1,0:T(8,128)(2,1)S(1)} %slice.151), channel_id=1, source_target_pairs={{0,1},{1,0},{2,3},{3,2},{4,5},{5,4},{6,7},{7,6},{8,9},{9,8},{10,11... | collective-permute-start | bytes 3145736 | tf_op jit(solution)/shard_map/ppermute | solution.py:63
  112.9 19.1 %copy-start.3 = (bf16[64,2048]{1,0:T(8,128)(2,1)S(1)}, bf16[64,2048]{1,0:T(8,128)(2,1)}, u32[]{:S(2)}) copy-start(bf16[64,2048]{1,0:T(8,128)(2,1)} %param.22) | copy-start | bytes 786436
  112.9 19.2 %copy-start.6 = (f32[2048]{0:T(1024)S(1)}, f32[2048]{0:T(1024)}, u32[]{:S(2)}) copy-start(f32[2048]{0:T(1024)} %param.23) | copy-start | bytes 24580
  148.3 6.8 %collective-permute-start.6 = (bf16[256,2048]{1,0:T(8,128)(2,1)S(1)}, bf16[256,2048]{1,0:T(8,128)(2,1)S(1)}, u32[]{:S(2)}, u32[]{:S(2)}) collective-permute-start(bf16[256,2048]{1,0:T(8,128)(2,1)S(1)} %bitcast.136), channel_id=1, source_target_pairs={{0,1},{1,0},{2,3},{3,2},{4,5},{5,4},{6,7},{7,6},{8,9},{9,8},{10,11... | collective-permute-start | bytes 3145736 | tf_op jit(solution)/shard_map/ppermute | solution.py:63
  187.9 21.3 %collective-permute-start.7 = (bf16[256,2048]{1,0:T(8,128)(2,1)S(1)}, bf16[256,2048]{1,0:T(8,128)(2,1)S(1)}, u32[]{:S(2)}, u32[]{:S(2)}) collective-permute-start(bf16[256,2048]{1,0:T(8,128)(2,1)S(1)} %slice.153), channel_id=1, source_target_pairs={{0,1},{1,0},{2,3},{3,2},{4,5},{5,4},{6,7},{7,6},{8,9},{9,8},{10,11... | collective-permute-start | bytes 3145736 | tf_op jit(solution)/shard_map/ppermute | solution.py:63
Sparse Core Ops, SparseCore 0:
  9.4 169.7 all-gather.1

commit v4 on v3

--- a/solution.py
+++ b/solution.py
@@ -1,9 +1,11 @@
+import functools
 import jax
 import jax.numpy as jnp
+import numpy as np
 from jax import lax
 from jax.experimental import pallas as pl
 from jax.experimental.pallas import tpu as pltpu
-from jax.sharding import PartitionSpec as P
+from jax.sharding import Mesh, PartitionSpec as P
 
 BLOCK = 128
 
@@ -13,8 +15,10 @@
 highest = lax.Precision.HIGHEST
 
 
-def gathered_weights(up, down, axis):
-    return lax.all_gather(jnp.concatenate([up, down.T], axis=1), axis, axis=0, tiled=True)
+def gathered_weights(up, down):
+    both = jnp.concatenate([up, down.T], axis=1)
+    whole = lax.all_gather(both, ("sp", "core"), axis=0, tiled=True)
+    return whole.reshape(lax.axis_size("sp"), lax.axis_size("core"), *both.shape)
 
 
 def shifted_on(x, axis, distance):
@@ -59,38 +63,33 @@
     return earlier
 
 
-def with_partner(x, axis):
-    return lax.ppermute(x, axis, [(k, k ^ 1) for k in range(lax.axis_size(axis))])
-
-
-def among_chips(blocks, axis):
-    length = lax.axis_size(axis)
-    groups = [list(range(core, length, 2)) for core in range(2)]
-    return lax.all_to_all(blocks, axis, 0, 0, tiled=True, axis_index_groups=groups)
-
-
-def own_core_first(x, axis):
-    chips = lax.axis_size(axis) // 2
-    core = lax.axis_index(axis) % 2
+def among_chips(blocks):
+    return lax.all_to_all(blocks, "chip", 0, 0, tiled=True)
+
+
+def own_core_first(x):
+    chips = lax.axis_size("chip")
+    core = lax.axis_index("core")
     blocks = x.reshape(chips, 2, -1, x.shape[-1])
     first = jnp.where(core == 0, blocks[:, 0], blocks[:, 1])
     second = jnp.where(core == 0, blocks[:, 1], blocks[:, 0])
     return jnp.concatenate([first, second], axis=0).reshape(x.shape)
 
 
-def sum_at_owner(rows, axis):
-    chips = lax.axis_size(axis) // 2
+def sum_of_cores(rows):
     half = rows.shape[0] // 2
-    found = with_partner(rows[half:], axis)
-    both = (rows[:half].astype(jnp.float32) + found.astype(jnp.float32)).astype(jnp.bfloat16)
-    blocks = among_chips(both.reshape(chips, -1, both.shape[-1]), axis)
+    found = lax.ppermute(rows[half:], "core", [(0, 1), (1, 0)])
+    return (rows[:half].astype(jnp.float32) + found.astype(jnp.float32)).astype(jnp.bfloat16)
+
+
+def sum_of_chips(rows):
+    blocks = among_chips(rows.reshape(lax.axis_size("chip"), -1, rows.shape[-1]))
     return jnp.sum(blocks.astype(jnp.float32), axis=0)
 
 
-def rows_of_all(x, axis):
-    chips = lax.axis_size(axis) // 2
-    own = among_chips(jnp.broadcast_to(x, (chips, *x.shape)), axis).reshape(-1, x.shape[-1])
-    return own, with_partner(own, axis)
+def rows_of_chips(x):
+    copies = jnp.broadcast_to(x, (lax.axis_size("chip"), *x.shape))
+    return among_chips(copies).reshape(-1, x.shape[-1])
 
 
 def rms_norm(tensor, gain_vec):
@@ -126,56 +125,64 @@
     return (*lax.optimization_barrier((spread(total), spread(top))), memory)
 
 
-def feed_forward_kernel(own_ref, other_ref, up_ref, down_ref, out_ref, active_ref):
+def feed_forward_kernel(ups, rows_ref, up_ref, down_ref, out_ref, active_ref):
     step = pl.program_id(0)
-    width = up_ref.shape[1]
-    ups = active_ref.shape[1] // width
-    half = own_ref.shape[0]
+    width = up_ref.shape[-1]
+    hidden = down_ref.shape[-1]
 
     @pl.when(step < ups)
     def _():
         cols = pl.ds(pl.multiple_of(step * width, width), width)
-        for k, rows_ref in enumerate((own_ref, other_ref)):
-            upward = jnp.dot(rows_ref[...], up_ref[...], preferred_element_type=jnp.float32)
-            active = jnp.square(jnp.maximum(upward, 0.0)).astype(jnp.bfloat16)
-            active_ref[k * half : (k + 1) * half, cols] = active
+        upward = jnp.dot(
+            rows_ref[...], up_ref[...].reshape(-1, width), preferred_element_type=jnp.float32
+        )
+        active_ref[:, cols] = jnp.square(jnp.maximum(upward, 0.0)).astype(jnp.bfloat16)
 
     @pl.when(step >= ups)
     def _():
-        out_ref[...] = lax.dot_general(
-            active_ref[...],
-            down_ref[...],
-            (((1,), (1,)), ((), ())),
-            preferred_element_type=jnp.float32,
-        ).astype(jnp.bfloat16)
-
-
-def feed_forward(own, other, weights, hidden):
-    half, features = own.shape
-    up_width, down_height = (hidden // 2, features // 4)
-    ups, downs = (hidden // up_width, features // down_height)
+        total = None
+        for core in range(down_ref.shape[1]):
+            part = lax.dot_general(
+                active_ref[:, core * hidden : (core + 1) * hidden],
+                down_ref[:, core].reshape(-1, hidden),
+                (((1,), (1,)), ((), ())),
+                preferred_element_type=jnp.float32,
+            )
+            total = part if total is None else total + part
+        out_ref[...] = total.astype(jnp.bfloat16)
+
+
+def feed_forward(rows, weights, hidden):
+    count, features = rows.shape
+    pieces, cores, height, _ = weights.shape
+    width, taken = (hidden, pieces // 2)
+    each = hidden // width
+    ups, downs = (cores * each, pieces // taken)
+    up_at = lambda i: jnp.minimum(i, ups - 1)
+    down_at = lambda i: jnp.maximum(i - ups, 0)
     return pl.pallas_call(
-        feed_forward_kernel,
+        functools.partial(feed_forward_kernel, ups),
         grid=(ups + downs,),
-        out_shape=jax.ShapeDtypeStruct((2 * half, features), jnp.bfloat16),
+        out_shape=jax.ShapeDtypeStruct((count, features), jnp.bfloat16),
         in_specs=[
-            pl.BlockSpec((half, features), lambda i: (0, 0)),
-            pl.BlockSpec((half, features), lambda i: (0, 0)),
-            pl.BlockSpec((features, up_width), lambda i: (0, jnp.minimum(i, ups - 1))),
-            pl.BlockSpec((down_height, hidden), lambda i: (jnp.maximum(i - ups, 0), 1)),
+            pl.BlockSpec((count, features), lambda i: (0, 0)),
+            pl.BlockSpec(
+                (pieces, 1, height, width), lambda i: (0, up_at(i) // each, 0, up_at(i) % each)
+            ),
+            pl.BlockSpec((taken, cores, height, hidden), lambda i: (down_at(i), 0, 0, 1)),
         ],
-        out_specs=pl.BlockSpec((2 * half, down_height), lambda i: (0, jnp.maximum(i - ups, 0))),
-        scratch_shapes=[pltpu.VMEM((2 * half, hidden), jnp.bfloat16)],
+        out_specs=pl.BlockSpec((count, taken * height), lambda i: (0, down_at(i))),
+        scratch_shapes=[pltpu.VMEM((count, cores * hidden), jnp.bfloat16)],
         compiler_params=pltpu.CompilerParams(
             dimension_semantics=("arbitrary",), vmem_limit_bytes=48 * 1024 * 1024
         ),
         cost_estimate=pl.CostEstimate(
-            flops=8 * half * features * hidden,
-            bytes_accessed=4 * features * hidden + 8 * half * features,
+            flops=4 * count * features * cores * hidden,
+            bytes_accessed=4 * features * cores * hidden + 4 * count * features,
             transcendentals=0,
         ),
         name="feed_forward",
-    )(own, other, weights, weights)
+    )(rows, weights, weights)
 
 
 def block_summary(key_blk, val_blk, gate_blk, decay_logarithm):
@@ -207,7 +214,7 @@
     head_dim = queries.shape[1] // head_count
     block_len = BLOCK
     block_count = tok_count // block_len
-    weights = gathered_weights(feedforward_up_matrix, feedforward_down_matrix, "sp")
+    weights = gathered_weights(feedforward_up_matrix, feedforward_down_matrix)
 
     def to_blocks(tensor):
         return (
@@ -261,34 +268,40 @@
         output_preactivation.astype(jnp.float32).reshape(tok_count, head_count, head_dim)
     )
     mixed = gated.reshape(tok_count, head_count * head_dim).astype(jnp.bfloat16)
-    mixed = own_core_first(mixed, "tp")
+    mixed = own_core_first(mixed)
     partial_branch = jnp.dot(
         mixed, output_projection_matrix, preferred_element_type=jnp.float32
     ).astype(jnp.bfloat16)
-    branch = sum_at_owner(partial_branch, "tp")
+    branch = sum_of_chips(sum_of_cores(partial_branch))
     mid_state = (residual.astype(jnp.float32) + branch).astype(jnp.bfloat16)
     normed = rms_norm(mid_state.astype(jnp.float32), feedforward_norm_gain).astype(jnp.bfloat16)
-    own, other = rows_of_all(normed, "tp")
-    mlp_rows = feed_forward(own, other, weights, feedforward_up_matrix.shape[1])
-    mlp_sum = sum_at_owner(mlp_rows, "tp")
-    return (mid_state.astype(jnp.float32) + mlp_sum).astype(jnp.bfloat16)
+    mlp_rows = feed_forward(rows_of_chips(normed), weights, feedforward_up_matrix.shape[1])
+    return (mid_state.astype(jnp.float32) + sum_of_chips(mlp_rows)).astype(jnp.bfloat16)
 
 
 def solution(mesh):
+    groups, places, lanes = mesh.devices.shape
+    split = Mesh(
+        np.asarray(mesh.devices).reshape(groups, places, lanes // 2, 2),
+        ("grp", "sp", "chip", "core"),
+    )
+    rows, heads = (("grp", "sp"), ("chip", "core"))
     in_specs = (
-        P(("grp", "sp"), "tp"),
-        P(("grp", "sp"), "tp"),
-        P(("grp", "sp"), "tp"),
-        P(("grp", "sp"), "tp"),
-        P("tp", ("grp", "sp")),
-        P("tp", ("grp", "sp")),
-        P("tp", ("grp", "sp")),
+        P(rows, heads),
+        P(rows, heads),
+        P(rows, heads),
+        P(rows, heads),
+        P(heads, rows),
+        P(heads, rows),
+        P(heads, rows),
         P(),
-        P("tp", None),
-        P(("grp", "sp", "tp"), None),
+        P(heads, None),
+        P((*rows, *heads), None),
         P(),
-        P("sp", "tp"),
-        P("tp", "sp"),
-    )
-    out_specs = P(("grp", "sp", "tp"), None)
-    return jax.shard_map(shards, mesh=mesh, in_specs=in_specs, out_specs=out_specs, check_vma=False)
+        P("sp", heads),
+        P(heads, "sp"),
+    )
+    out_specs = P((*rows, *heads), None)
+    return jax.shard_map(
+        shards, mesh=split, in_specs=in_specs, out_specs=out_specs, check_vma=False
+    )

time: 236 us -> 233 us (0.987)
  starting transfers between devices: 109 us -> 85.7 us
  waiting for transfers between devices: 36.1 us -> 55.6 us
    all_gather x1, waiting for transfers between devices: 24.1 us -> 48.2 us  [gathered_weights(): whole = lax.all_gather(both, ('sp', 'core'), axis=0, tiled=True)]
    ppermute x3 -> x1, starting transfers between devices: 30.3 us -> 6.96 us  [sum_of_cores(): found = lax.ppermute(rows[half:], 'core', [(0, 1), (1, 0)])]
    ppermute x3 -> x1, waiting for transfers between devices: 6.79 us -> 2.45 us  [sum_of_cores(): found = lax.ppermute(rows[half:], 'core', [(0, 1), (1, 0)])]
  transfers between devices with their start and end apart: 9 -> 7, of which waited for: 9 -> 7; matrix products, arithmetic and copies ran while one was open for 5% -> 5% of each run, Pallas kernels for 0% -> 0%
where the time goes in v4:
time: 233 us
  starting transfers between devices  85.7 us (37%)
  waiting for transfers between devices  55.6 us (24%)
  blocking collectives  53.5 us (23%)
  between operations  14 us (6%)
  other arithmetic  9.69 us (4%)
  Pallas kernels  9.6 us (4%)
  matrix products  3.6 us (2%)
    ppermute x5, starting transfers between devices, shifted_on(): lax.ppermute(x, axis, [(k, k + distance) for k in range(length - distance)])  78.7 us
    all_to_all x3, blocking collectives, among_chips(): return lax.all_to_all(blocks, 'chip', 0, 0, tiled=True)  53.5 us
    all_gather x1, waiting for transfers between devices, gathered_weights(): whole = lax.all_gather(both, ('sp', 'core'), axis=0, tiled=True)  48.2 us
    pallas_call x1, Pallas kernels, feed_forward(): pl.pallas_call(functools.partial(feed_forward_kernel, ups), grid=(ups + d...  9.6 us
    ppermute x1, starting transfers between devices, sum_of_cores(): found = lax.ppermute(rows[half:], 'core', [(0, 1), (1, 0)])  6.96 us
    ppermute x5, waiting for transfers between devices, shifted_on(): lax.ppermute(x, axis, [(k, k + distance) for k in range(length - distance)])  4.84 us
  transfers between devices with their start and end apart: 7, of which 7 were waited for; matrix products, arithmetic and copies ran while one was open for 5% of the time, Pallas kernels for 0%

profile of v4, /device:TPU:33, one launch (start us, length us, event | category | flops | bytes accessed | tf_op | source)
XLA Modules:
  0.0 232.8 jit_solution(4939786598767673566)
XLA Ops:
  6.5 0.0 copy-start
  6.6 0.0 all-gather.2.cloned.1.call-start
  6.6 1.7 pad_maximum_fusion
  8.3 0.1 all-gather.2.cloned.1.call-update
  8.4 0.7 fusion.45
  9.1 1.2 reduce_window_sum.11
  10.3 0.2 slice_reduce_fusion.12
  10.5 0.9 fusion.44
  11.4 0.1 select_reduce_fusion.1
  11.5 0.1 fusion.43
  11.5 0.1 fusion.46
  11.6 0.1 fusion.42
  11.7 0.1 copy.34
  11.8 0.8 subtract_exponential_fusion.1
  12.6 0.9 convert_multiply_fusion.2
  13.5 1.6 fusion.13
  15.1 0.0 copy-start.2
  15.1 0.2 multiply_reduce_fusion
  15.3 0.0 copy-start.1
  15.3 0.2 slice_reduce_fusion
  15.6 5.2 %collective-permute-start = (bf16[1,144,128]{2,1,0:T(8,128)(2,1)S(1)}, bf16[1,144,128]{2,1,0:T(8,128)(2,1)S(1)}, u32[]{:S(2)}, u32[]{:S(2)}) collective-permute-start(bf16[1,144,128]{2,1,0:T(8,128)(2,1)S(1)} %fusion.30), channel_id=1, source_target_pairs={{0,8},{8,16},{16,24},{24,32},{32,40},{40,48},{48,56},{56,64},{64,7... | collective-permute-start | bytes 110600 | tf_op jit(solution)/shard_map/ppermute | solution.py:26
  20.8 1.0 collective-permute-done
  22.0 6.6 %collective-permute-start.1 = (bf16[1,144,128]{2,1,0:T(8,128)(2,1)S(1)}, bf16[1,144,128]{2,1,0:T(8,128)(2,1)S(1)}, u32[]{:S(2)}, u32[]{:S(2)}) collective-permute-start(bf16[1,144,128]{2,1,0:T(8,128)(2,1)S(1)} %fusion.31), channel_id=1, source_target_pairs={{0,16},{8,24},{16,32},{24,40},{32,48},{40,56},{48,64},{56,72},{64,... | collective-permute-start | bytes 110600 | tf_op jit(solution)/shard_map/ppermute | solution.py:26
  28.7 1.0 collective-permute-done.1
  29.9 12.4 %collective-permute-start.2 = (bf16[1,144,128]{2,1,0:T(8,128)(2,1)S(1)}, bf16[1,144,128]{2,1,0:T(8,128)(2,1)S(1)}, u32[]{:S(2)}, u32[]{:S(2)}) collective-permute-start(bf16[1,144,128]{2,1,0:T(8,128)(2,1)S(1)} %fusion.32), channel_id=1, source_target_pairs={{0,32},{8,40},{16,48},{24,56},{32,64},{40,72},{48,80},{56,88},{64,... | collective-permute-start | bytes 110600 | tf_op jit(solution)/shard_map/ppermute | solution.py:26
  42.3 1.0 collective-permute-done.2
  43.5 0.0 copy-start.4
  43.5 0.0 copy-start.7
  43.6 22.9 %collective-permute-start.3 = (bf16[1,144,128]{2,1,0:T(8,128)(2,1)S(1)}, bf16[1,144,128]{2,1,0:T(8,128)(2,1)S(1)}, u32[]{:S(2)}, u32[]{:S(2)}) collective-permute-start(bf16[1,144,128]{2,1,0:T(8,128)(2,1)S(1)} %fusion.33), channel_id=1, source_target_pairs={{0,64},{8,72},{16,80},{24,88},{32,96},{40,104},{48,112},{56,120},{... | collective-permute-start | bytes 110600 | tf_op jit(solution)/shard_map/ppermute | solution.py:26
  66.5 0.1 copy.33
  66.6 0.9 collective-permute-done.3
  67.6 31.6 %collective-permute-start.4 = (bf16[1,144,128]{2,1,0:T(8,128)(2,1)S(1)}, bf16[1,144,128]{2,1,0:T(8,128)(2,1)S(1)}, u32[]{:S(2)}, u32[]{:S(2)}) collective-permute-start(bf16[1,144,128]{2,1,0:T(8,128)(2,1)S(1)} %fusion.34), channel_id=1, source_target_pairs={{0,128},{8,136},{16,144},{24,152},{32,160},{40,168},{48,176},{56,1... | collective-permute-start | bytes 110600 | tf_op jit(solution)/shard_map/ppermute | solution.py:26
  99.2 0.0 copy-done.5
  99.2 0.2 select_reduce_fusion
  99.5 0.8 collective-permute-done.4
  100.4 0.1 exponential_bitcast_fusion.1
  100.5 0.1 copy.38
  100.5 0.1 copy.37
  100.6 0.1 subtract_exponential_fusion
  100.8 0.0 copy-done.2
  100.8 0.4 fusion.2
  101.2 0.0 copy-done.1
  101.2 0.4 fusion.93
  101.6 0.5 multiply_reduce_fusion.1
  102.1 0.0 copy-done.4
  102.2 0.1 fusion.11
  102.4 0.7 convolution_convert_fusion
  103.1 0.1 slice.143
  103.2 7.0 %collective-permute-start.5 = (bf16[256,2048]{1,0:T(8,128)(2,1)S(1)}, bf16[256,2048]{1,0:T(8,128)(2,1)S(1)}, u32[]{:S(2)}, u32[]{:S(2)}) collective-permute-start(bf16[256,2048]{1,0:T(8,128)(2,1)S(1)} %slice.143), channel_id=1, source_target_pairs={{0,1},{1,0},{2,3},{3,2},{4,5},{5,4},{6,7},{7,6},{8,9},{9,8},{10,11... | collective-permute-start | bytes 3145736 | tf_op jit(solution)/shard_map/ppermute | solution.py:81
  110.2 2.5 %collective-permute-done.5 = bf16[256,2048]{1,0:T(8,128)(2,1)S(1)} collective-permute-done((bf16[256,2048]{1,0:T(8,128)(2,1)S(1)}, bf16[256,2048]{1,0:T(8,128)(2,1)S(1)}, u32[]{:S(2)}, u32[]{:S(2)}) %collective-permute-start.5) | collective-permute-done | bytes 1048608 | tf_op jit(solution)/shard_map/ppermute | solution.py:81
  112.6 0.4 add_convert_fusion
  113.0 0.0 copy-start.3
  113.0 0.0 copy-start.6
  113.0 18.8 %all_to_all.15 = bf16[4,64,2048]{2,1,0:T(8,128)(2,1)S(1)} all-to-all(bf16[4,64,2048]{2,1,0:T(8,128)(2,1)S(1)} %bitcast.141), channel_id=1, replica_groups=mesh['grp'=2,'sp'=32,'chip'=4,'core'=2] {'chip'}, dimensions={0} | all-to-all | bytes 2097152 | tf_op jit(solution)/shard_map/all_to_all | solution.py:67
  131.8 0.2 convert_reduce_fusion.1
  132.0 0.2 fusion.3
  132.2 0.1 fusion.5
  132.3 0.1 broadcast_in_dim.106
  132.4 15.9 %all_to_all.16 = bf16[4,64,2048]{2,1,0:T(8,128)(2,1)S(1)} all-to-all(bf16[4,64,2048]{2,1,0:T(8,128)(2,1)S(1)} %broadcast_in_dim.106), channel_id=1, replica_groups=mesh['grp'=2,'sp'=32,'chip'=4,'core'=2] {'chip'}, dimensions={0} | all-to-all | bytes 2097152 | tf_op jit(solution)/shard_map/all_to_all | solution.py:67
  148.3 48.2 %all-gather.2.cloned.1.call-done = bf16[4096,2048]{1,0:T(8,128)(2,1)} async-done(((bf16[64,2048]{1,0:T(8,128)(2,1)}), bf16[4096,2048]{1,0:T(8,128)(2,1)}) %all-gather.2.cloned.1.call-update) | async-done | bytes 16777232 | tf_op jit(solution)/shard_map/all_gather | solution.py:20
  196.5 9.6 %feed_forward.1 = bf16[256,2048]{1,0:T(8,128)(2,1)S(1)} custom-call(bf16[256,2048]{1,0:T(8,128)(2,1)S(1)} %bitcast.137, bf16[32,2,64,2048]{3,2,1,0:T(8,128)(2,1)} %bitcast.139, bf16[32,2,64,2048]{3,2,1,0:T(8,128)(2,1)} %bitcast.140), custom_call_target="tpu_custom_call" | custom-call | flops 4294967296 | bytes 18874368 | tf_op jit(solution)/shard_map/feed_forward/pallas_call | solution.py:163
  206.1 18.9 %all_to_all.17 = bf16[4,64,2048]{2,1,0:T(8,128)(2,1)S(1)} all-to-all(bf16[4,64,2048]{2,1,0:T(8,128)(2,1)S(1)} %bitcast.138), channel_id=1, replica_groups=mesh['grp'=2,'sp'=32,'chip'=4,'core'=2] {'chip'}, dimensions={0} | all-to-all | bytes 2097152 | tf_op jit(solution)/shard_map/all_to_all | solution.py:67
  225.0 0.2 convert_reduce_fusion
  225.2 0.8 fusion.6
  (65 shorter events, 0.8 us)
Async XLA Ops:
  6.5 95.8 %copy-start = (bf16[128,2048]{1,0:T(8,128)(2,1)S(1)}, bf16[128,2048]{1,0:T(8,128)(2,1)}, u32[]{:S(2)}) copy-start(bf16[128,2048]{1,0:T(8,128)(2,1)} %param.21) | copy-start | bytes 1572868
  6.6 190.0 %all-gather.2.cloned.1.call-start = ((), (), s32[]{:S(2)}) async-start(), calls=%async_computation.3 | async-start | bytes 17039360 | tf_op jit(solution)/shard_map/all_gather | solution.py:20
  8.3 90.9 %copy-start.5 = (f32[1,512]{1,0:T(1,128)S(1)}, f32[1,512]{1,0:T(1,128)}, u32[]{:S(2)}) copy-start(f32[1,512]{1,0:T(1,128)} %param.17) | copy-start | bytes 6148
  15.1 85.7 %copy-start.2 = (bf16[512,128]{1,0:T(8,128)(2,1)S(1)}, bf16[512,128]{1,0:T(8,128)(2,1)}, u32[]{:S(2)}) copy-start(bf16[512,128]{1,0:T(8,128)(2,1)} %param.13) | copy-start | bytes 393220
  15.3 85.9 %copy-start.1 = (bf16[512,128]{1,0:T(8,128)(2,1)S(1)}, bf16[512,128]{1,0:T(8,128)(2,1)}, u32[]{:S(2)}) copy-start(bf16[512,128]{1,0:T(8,128)(2,1)} %param.15) | copy-start | bytes 393220
  15.6 6.3 %collective-permute-start = (bf16[1,144,128]{2,1,0:T(8,128)(2,1)S(1)}, bf16[1,144,128]{2,1,0:T(8,128)(2,1)S(1)}, u32[]{:S(2)}, u32[]{:S(2)}) collective-permute-start(bf16[1,144,128]{2,1,0:T(8,128)(2,1)S(1)} %fusion.30), channel_id=1, source_target_pairs={{0,8},{8,16},{16,24},{24,32},{32,40},{40,48},{48,56},{56,64},{64,7... | collective-permute-start | bytes 110600 | tf_op jit(solution)/shard_map/ppermute | solution.py:26
  22.0 7.7 %collective-permute-start.1 = (bf16[1,144,128]{2,1,0:T(8,128)(2,1)S(1)}, bf16[1,144,128]{2,1,0:T(8,128)(2,1)S(1)}, u32[]{:S(2)}, u32[]{:S(2)}) collective-permute-start(bf16[1,144,128]{2,1,0:T(8,128)(2,1)S(1)} %fusion.31), channel_id=1, source_target_pairs={{0,16},{8,24},{16,32},{24,40},{32,48},{40,56},{48,64},{56,72},{64,... | collective-permute-start | bytes 110600 | tf_op jit(solution)/shard_map/ppermute | solution.py:26
  29.9 13.5 %collective-permute-start.2 = (bf16[1,144,128]{2,1,0:T(8,128)(2,1)S(1)}, bf16[1,144,128]{2,1,0:T(8,128)(2,1)S(1)}, u32[]{:S(2)}, u32[]{:S(2)}) collective-permute-start(bf16[1,144,128]{2,1,0:T(8,128)(2,1)S(1)} %fusion.32), channel_id=1, source_target_pairs={{0,32},{8,40},{16,48},{24,56},{32,64},{40,72},{48,80},{56,88},{64,... | collective-permute-start | bytes 110600 | tf_op jit(solution)/shard_map/ppermute | solution.py:26
  43.5 58.6 %copy-start.4 = (bf16[512,128]{1,0:T(8,128)(2,1)S(1)}, bf16[512,128]{1,0:T(8,128)(2,1)}, u32[]{:S(2)}) copy-start(bf16[512,128]{1,0:T(8,128)(2,1)} %param.16) | copy-start | bytes 393220
  43.5 58.6 %copy-start.7 = (f32[128]{0:T(128)S(1)}, f32[128]{0:T(128)}, u32[]{:S(2)}) copy-start(f32[128]{0:T(128)} %param.20) | copy-start | bytes 1540
  43.6 23.9 %collective-permute-start.3 = (bf16[1,144,128]{2,1,0:T(8,128)(2,1)S(1)}, bf16[1,144,128]{2,1,0:T(8,128)(2,1)S(1)}, u32[]{:S(2)}, u32[]{:S(2)}) collective-permute-start(bf16[1,144,128]{2,1,0:T(8,128)(2,1)S(1)} %fusion.33), channel_id=1, source_target_pairs={{0,64},{8,72},{16,80},{24,88},{32,96},{40,104},{48,112},{56,120},{... | collective-permute-start | bytes 110600 | tf_op jit(solution)/shard_map/ppermute | solution.py:26
  67.6 32.7 %collective-permute-start.4 = (bf16[1,144,128]{2,1,0:T(8,128)(2,1)S(1)}, bf16[1,144,128]{2,1,0:T(8,128)(2,1)S(1)}, u32[]{:S(2)}, u32[]{:S(2)}) collective-permute-start(bf16[1,144,128]{2,1,0:T(8,128)(2,1)S(1)} %fusion.34), channel_id=1, source_target_pairs={{0,128},{8,136},{16,144},{24,152},{32,160},{40,168},{48,176},{56,1... | collective-permute-start | bytes 110600 | tf_op jit(solution)/shard_map/ppermute | solution.py:26
  103.2 9.4 %collective-permute-start.5 = (bf16[256,2048]{1,0:T(8,128)(2,1)S(1)}, bf16[256,2048]{1,0:T(8,128)(2,1)S(1)}, u32[]{:S(2)}, u32[]{:S(2)}) collective-permute-start(bf16[256,2048]{1,0:T(8,128)(2,1)S(1)} %slice.143), channel_id=1, source_target_pairs={{0,1},{1,0},{2,3},{3,2},{4,5},{5,4},{6,7},{7,6},{8,9},{9,8},{10,11... | collective-permute-start | bytes 3145736 | tf_op jit(solution)/shard_map/ppermute | solution.py:81
  113.0 18.9 %copy-start.3 = (bf16[64,2048]{1,0:T(8,128)(2,1)S(1)}, bf16[64,2048]{1,0:T(8,128)(2,1)}, u32[]{:S(2)}) copy-start(bf16[64,2048]{1,0:T(8,128)(2,1)} %param.22) | copy-start | bytes 786436
  113.0 19.1 %copy-start.6 = (f32[2048]{0:T(1024)S(1)}, f32[2048]{0:T(1024)}, u32[]{:S(2)}) copy-start(f32[2048]{0:T(1024)} %param.23) | copy-start | bytes 24580
Sparse Core Ops, SparseCore 0:
  9.5 187.0 all-gather.1

commit v5 on v4

--- a/solution.py
+++ b/solution.py
@@ -21,11 +21,6 @@
     return whole.reshape(lax.axis_size("sp"), lax.axis_size("core"), *both.shape)
 
 
-def shifted_on(x, axis, distance):
-    length = lax.axis_size(axis)
-    return lax.ppermute(x, axis, [(k, k + distance) for k in range(length - distance)])
-
-
 def bf16_parts(x):
     parts = []
     for _ in range(3):
@@ -50,17 +45,28 @@
     return (total, jnp.where(present, top, neg_big), both[:, :head_dim])
 
 
-def prefix_by_doubling(part, axis):
+def state_before(part, axis):
     place = lax.axis_index(axis)
     length = lax.axis_size(axis)
     head_dim = part[2].shape[-1]
-    window, earlier, distance = (part, None, 1)
-    while distance < length:
-        found = unpacked(shifted_on(packed(window), axis, distance), head_dim, place >= distance)
-        earlier = found if earlier is None else combine(found, earlier)
-        window = combine(found, window)
+
+    def fetched(window, distance, ends):
+        pairs = [(end - distance, end) for end in ends]
+        stride = ends[1] - ends[0] if len(ends) > 1 else length
+        present = (place >= ends[0]) & (lax.rem(place - ends[0] + length, stride) == 0)
+        return unpacked(lax.ppermute(packed(window), axis, pairs), head_dim, present)
+
+    window, distance = (part, 1)
+    while 2 * distance < length:
+        ends = list(range(2 * distance - 1, length, 2 * distance))
+        window = combine(fetched(window, distance, ends), window)
         distance *= 2
-    return earlier
+    distance //= 2
+    while distance >= 1:
+        ends = list(range(3 * distance - 1, length, 2 * distance))
+        window = combine(fetched(window, distance, ends), window)
+        distance //= 2
+    return fetched(window, 1, list(range(1, length)))
 
 
 def among_chips(blocks):
@@ -125,64 +131,77 @@
     return (*lax.optimization_barrier((spread(total), spread(top))), memory)
 
 
-def feed_forward_kernel(ups, rows_ref, up_ref, down_ref, out_ref, active_ref):
-    step = pl.program_id(0)
-    width = up_ref.shape[-1]
-    hidden = down_ref.shape[-1]
-
-    @pl.when(step < ups)
-    def _():
-        cols = pl.ds(pl.multiple_of(step * width, width), width)
+def feed_forward_kernel(hidden, rows_ref, weights_ref, out_ref, up_buf, down_buf, active_ref, sems):
+    pieces, height, width = up_buf.shape[1:]
+    taken, cores = down_buf.shape[1:3]
+    ups, downs = (up_buf.shape[0], down_buf.shape[0])
+    each = hidden // width
+    copies = [
+        pltpu.make_async_copy(
+            weights_ref.at[:, k // each, :, pl.ds(k % each * width, width)],
+            up_buf.at[k],
+            sems.at[k],
+        )
+        for k in range(ups)
+    ] + [
+        pltpu.make_async_copy(
+            weights_ref.at[pl.ds(k * taken, taken), :, :, pl.ds(hidden, hidden)],
+            down_buf.at[k],
+            sems.at[ups + k],
+        )
+        for k in range(downs)
+    ]
+    for copy in copies:
+        copy.start()
+    rows = rows_ref[...]
+    for k in range(ups):
+        copies[k].wait()
         upward = jnp.dot(
-            rows_ref[...], up_ref[...].reshape(-1, width), preferred_element_type=jnp.float32
+            rows, up_buf[k].reshape(-1, width), preferred_element_type=jnp.float32
         )
-        active_ref[:, cols] = jnp.square(jnp.maximum(upward, 0.0)).astype(jnp.bfloat16)
-
-    @pl.when(step >= ups)
-    def _():
+        active = jnp.square(jnp.maximum(upward, 0.0)).astype(jnp.bfloat16)
+        active_ref[:, k * width : (k + 1) * width] = active
+    for k in range(downs):
+        copies[ups + k].wait()
         total = None
-        for core in range(down_ref.shape[1]):
+        for core in range(cores):
             part = lax.dot_general(
                 active_ref[:, core * hidden : (core + 1) * hidden],
-                down_ref[:, core].reshape(-1, hidden),
+                down_buf[k, :, core].reshape(-1, hidden),
                 (((1,), (1,)), ((), ())),
                 preferred_element_type=jnp.float32,
             )
             total = part if total is None else total + part
-        out_ref[...] = total.astype(jnp.bfloat16)
+        out_ref[:, k * taken * height : (k + 1) * taken * height] = total.astype(jnp.bfloat16)
 
 
 def feed_forward(rows, weights, hidden):
     count, features = rows.shape
     pieces, cores, height, _ = weights.shape
-    width, taken = (hidden, pieces // 2)
-    each = hidden // width
-    ups, downs = (cores * each, pieces // taken)
-    up_at = lambda i: jnp.minimum(i, ups - 1)
-    down_at = lambda i: jnp.maximum(i - ups, 0)
+    width, taken = (hidden // 2, pieces // 4)
+    ups, downs = (cores * hidden // width, pieces // taken)
     return pl.pallas_call(
-        functools.partial(feed_forward_kernel, ups),
-        grid=(ups + downs,),
+        functools.partial(feed_forward_kernel, hidden),
         out_shape=jax.ShapeDtypeStruct((count, features), jnp.bfloat16),
         in_specs=[
-            pl.BlockSpec((count, features), lambda i: (0, 0)),
-            pl.BlockSpec(
-                (pieces, 1, height, width), lambda i: (0, up_at(i) // each, 0, up_at(i) % each)
-            ),
-            pl.BlockSpec((taken, cores, height, hidden), lambda i: (down_at(i), 0, 0, 1)),
+            pl.BlockSpec(memory_space=pltpu.VMEM),
+            pl.BlockSpec(memory_space=pl.ANY),
         ],
-        out_specs=pl.BlockSpec((count, taken * height), lambda i: (0, down_at(i))),
-        scratch_shapes=[pltpu.VMEM((count, cores * hidden), jnp.bfloat16)],
-        compiler_params=pltpu.CompilerParams(
-            dimension_semantics=("arbitrary",), vmem_limit_bytes=48 * 1024 * 1024
-        ),
+        out_specs=pl.BlockSpec(memory_space=pltpu.VMEM),
+        scratch_shapes=[
+            pltpu.VMEM((ups, pieces, height, width), jnp.bfloat16),
+            pltpu.VMEM((downs, taken, cores, height, hidden), jnp.bfloat16),
+            pltpu.VMEM((count, cores * hidden), jnp.bfloat16),
+            pltpu.SemaphoreType.DMA((ups + downs,)),
+        ],
+        compiler_params=pltpu.CompilerParams(vmem_limit_bytes=48 * 1024 * 1024),
         cost_estimate=pl.CostEstimate(
             flops=4 * count * features * cores * hidden,
             bytes_accessed=4 * features * cores * hidden + 4 * count * features,
             transcendentals=0,
         ),
         name="feed_forward",
-    )(rows, weights, weights)
+    )(rows, weights)
 
 
 def block_summary(key_blk, val_blk, gate_blk, decay_logarithm):
@@ -236,7 +255,7 @@
     summaries = block_summary(key_blk, val_blk, gate_blk, decay_logarithm)
     prefix_total, prefix_top, prefix_memory = block_prefixes(*summaries)
     whole = (prefix_total[-1], prefix_top[-1], prefix_memory[-1])
-    before_total, before_top, before_memory = prefix_by_doubling(whole, "sp")
+    before_total, before_top, before_memory = state_before(whole, "sp")
     incoming_top = jnp.maximum(before_total, before_top)
     incoming_memory = jnp.exp(before_top - incoming_top) * before_memory
     carried = prefix_total[:-1] + incoming_top

time: 233 us -> 222 us (0.953)
  starting transfers between devices: 85.7 us -> 60.1 us
  waiting for transfers between devices: 55.6 us -> 72.3 us
    ppermute x5 -> x9, starting transfers between devices: 78.7 us -> 22.2 us  [fetched(): lax.ppermute(packed(window), axis, pairs)]
    ppermute x1, starting transfers between devices: 6.96 us -> 37.9 us  [sum_of_cores(): found = lax.ppermute(rows[half:], 'core', [(0, 1), (1, 0)])]
    all_gather x1, waiting for transfers between devices: 48.2 us -> 68 us  [gathered_weights(): whole = lax.all_gather(both, ('sp', 'core'), axis=0, tiled=True)]
    ppermute x5 -> x9, waiting for transfers between devices: 4.84 us -> 1.83 us  [fetched(): lax.ppermute(packed(window), axis, pairs)]
  transfers between devices with their start and end apart: 7 -> 11, of which waited for: 7 -> 4; matrix products, arithmetic and copies ran while one was open for 5% -> 6% of each run, Pallas kernels for 0% -> 0%
where the time goes in v5:
time: 222 us; the launch traced here: 221 us
  waiting for transfers between devices  72.3 us (33%)
  starting transfers between devices  60.1 us (27%)
  blocking collectives  52.1 us (23%)
  between operations  14.4 us (6%)
  other arithmetic  10 us (5%)
  Pallas kernels  7.5 us (3%)
  matrix products  3.59 us (2%)
    all_gather x1, waiting for transfers between devices, gathered_weights(): whole = lax.all_gather(both, ('sp', 'core'), axis=0, tiled=True)  68 us
    all_to_all x3, blocking collectives, among_chips(): return lax.all_to_all(blocks, 'chip', 0, 0, tiled=True)  52.1 us
    ppermute x1, starting transfers between devices, sum_of_cores(): found = lax.ppermute(rows[half:], 'core', [(0, 1), (1, 0)])  37.9 us
    ppermute x9, starting transfers between devices, fetched(): lax.ppermute(packed(window), axis, pairs)  22.2 us
    pallas_call x1, Pallas kernels, feed_forward(): pl.pallas_call(functools.partial(feed_forward_kernel, hidden), out_shape=...  7.5 us
  transfers between devices with their start and end apart: 11, of which 4 were waited for; matrix products, arithmetic and copies ran while one was open for 6% of the time, Pallas kernels for 0%

profile of v5, /device:TPU:33, one launch (start us, length us, event | category | flops | bytes accessed | tf_op | source)
XLA Modules:
  0.0 221.3 jit_solution(2939427814614385629)
XLA Ops:
  6.6 1.7 pad_maximum_fusion
  8.3 0.1 all-gather.2.cloned.1.call-update
  8.4 0.7 fusion.62
  9.1 1.2 reduce_window_sum.11
  10.3 0.2 slice_reduce_fusion.20
  10.5 0.9 fusion.61
  11.4 0.1 select_reduce_fusion.1
  11.4 0.1 fusion.60
  11.5 0.1 fusion.63
  11.6 0.1 fusion.59
  11.7 0.1 copy.34
  11.8 0.8 subtract_exponential_fusion.1
  12.6 0.9 convert_multiply_fusion.2
  13.5 1.6 fusion.13
  15.1 0.2 multiply_reduce_fusion
  15.3 0.0 copy-start.5
  15.3 0.2 slice_reduce_fusion
  15.5 5.2 %collective-permute-start = (bf16[1,144,128]{2,1,0:T(8,128)(2,1)S(1)}, bf16[1,144,128]{2,1,0:T(8,128)(2,1)S(1)}, u32[]{:S(2)}, u32[]{:S(2)}) collective-permute-start(bf16[1,144,128]{2,1,0:T(8,128)(2,1)S(1)} %fusion.41), channel_id=1, source_target_pairs={{0,8},{16,24},{32,40},{48,56},{64,72},{80,88},{96,104},{112,120},{... | collective-permute-start | bytes 110600 | tf_op jit(solution)/shard_map/ppermute | solution.py:57
  20.8 1.0 collective-permute-done
  22.0 0.7 collective-permute-start.1
  22.7 0.0 copy-start.2
  22.9 0.7 collective-permute-start.2
  23.8 0.0 copy-start.1
  23.8 0.8 collective-permute-start.3
  24.6 0.0 collective-permute-done.3
  24.8 0.7 collective-permute-start.4
  25.7 0.7 collective-permute-start.5
  26.4 0.0 collective-permute-done.5
  26.6 0.7 collective-permute-start.6
  27.3 0.0 copy-start.4
  27.3 0.0 copy-start.7
  27.3 0.0 collective-permute-done.6
  27.5 0.7 collective-permute-start.7
  28.2 0.1 copy.33
  28.3 0.0 collective-permute-done.7
  28.5 12.2 %collective-permute-start.8 = (bf16[1,144,128]{2,1,0:T(8,128)(2,1)S(1)}, bf16[1,144,128]{2,1,0:T(8,128)(2,1)S(1)}, u32[]{:S(2)}, u32[]{:S(2)}) collective-permute-start(bf16[1,144,128]{2,1,0:T(8,128)(2,1)S(1)} %fusion.49), channel_id=1, source_target_pairs={{0,8},{8,16},{16,24},{24,32},{32,40},{40,48},{48,56},{56,64},{64,7... | collective-permute-start | bytes 110600 | tf_op jit(solution)/shard_map/ppermute | solution.py:57
  40.7 0.2 select_reduce_fusion
  40.9 0.8 collective-permute-done.8
  41.8 0.1 exponential_bitcast_fusion.1
  41.9 0.1 copy.38
  41.9 0.1 copy.37
  42.0 0.1 subtract_exponential_fusion
  42.2 0.4 fusion.2
  42.6 0.4 fusion.140
  43.0 0.5 multiply_reduce_fusion.1
  43.5 0.1 fusion.11
  43.7 0.7 convolution_convert_fusion
  44.4 0.1 slice.203
  44.5 37.9 %collective-permute-start.9 = (bf16[256,2048]{1,0:T(8,128)(2,1)S(1)}, bf16[256,2048]{1,0:T(8,128)(2,1)S(1)}, u32[]{:S(2)}, u32[]{:S(2)}) collective-permute-start(bf16[256,2048]{1,0:T(8,128)(2,1)S(1)} %slice.203), channel_id=1, source_target_pairs={{0,1},{1,0},{2,3},{3,2},{4,5},{5,4},{6,7},{7,6},{8,9},{9,8},{10,11... | collective-permute-start | bytes 3145736 | tf_op jit(solution)/shard_map/ppermute | solution.py:87
  82.5 2.4 %collective-permute-done.9 = bf16[256,2048]{1,0:T(8,128)(2,1)S(1)} collective-permute-done((bf16[256,2048]{1,0:T(8,128)(2,1)S(1)}, bf16[256,2048]{1,0:T(8,128)(2,1)S(1)}, u32[]{:S(2)}, u32[]{:S(2)}) %collective-permute-start.9) | collective-permute-done | bytes 1048608 | tf_op jit(solution)/shard_map/ppermute | solution.py:87
  84.9 0.4 add_convert_fusion
  85.3 0.0 copy-start.3
  85.3 0.0 copy-start.6
  85.3 17.4 %all_to_all.15 = bf16[4,64,2048]{2,1,0:T(8,128)(2,1)S(1)} all-to-all(bf16[4,64,2048]{2,1,0:T(8,128)(2,1)S(1)} %bitcast.172), channel_id=1, replica_groups=mesh['grp'=2,'sp'=32,'chip'=4,'core'=2] {'chip'}, dimensions={0} | all-to-all | bytes 2097152 | tf_op jit(solution)/shard_map/all_to_all | solution.py:73
  102.7 0.2 convert_reduce_fusion.1
  102.9 0.2 fusion.3
  103.1 0.1 fusion.5
  103.2 0.1 broadcast_in_dim.118
  103.3 16.4 %all_to_all.16 = bf16[4,64,2048]{2,1,0:T(8,128)(2,1)S(1)} all-to-all(bf16[4,64,2048]{2,1,0:T(8,128)(2,1)S(1)} %broadcast_in_dim.118), channel_id=1, replica_groups=mesh['grp'=2,'sp'=32,'chip'=4,'core'=2] {'chip'}, dimensions={0} | all-to-all | bytes 2097152 | tf_op jit(solution)/shard_map/all_to_all | solution.py:73
  119.7 68.0 %all-gather.2.cloned.1.call-done = bf16[4096,2048]{1,0:T(8,128)(2,1)} async-done(((bf16[64,2048]{1,0:T(8,128)(2,1)}), bf16[4096,2048]{1,0:T(8,128)(2,1)}) %all-gather.2.cloned.1.call-update) | async-done | bytes 16777232 | tf_op jit(solution)/shard_map/all_gather | solution.py:20
  187.8 7.5 %feed_forward.1 = bf16[256,2048]{1,0:T(8,128)(2,1)S(1)} custom-call(bf16[256,2048]{1,0:T(8,128)(2,1)S(1)} %bitcast.169, bf16[32,2,64,2048]{3,2,1,0:T(8,128)(2,1)} %bitcast.171), custom_call_target="tpu_custom_call" | custom-call | flops 4294967296 | bytes 18874368 | tf_op jit(solution)/shard_map/feed_forward/pallas_call | solution.py:183
  195.3 18.2 %all_to_all.17 = bf16[4,64,2048]{2,1,0:T(8,128)(2,1)S(1)} all-to-all(bf16[4,64,2048]{2,1,0:T(8,128)(2,1)S(1)} %bitcast.170), channel_id=1, replica_groups=mesh['grp'=2,'sp'=32,'chip'=4,'core'=2] {'chip'}, dimensions={0} | all-to-all | bytes 2097152 | tf_op jit(solution)/shard_map/all_to_all | solution.py:73
  213.5 0.2 convert_reduce_fusion
  213.7 0.8 fusion.6
  (111 shorter events, 1.3 us)
Async XLA Ops:
  6.5 37.2 %copy-start = (bf16[128,2048]{1,0:T(8,128)(2,1)S(1)}, bf16[128,2048]{1,0:T(8,128)(2,1)}, u32[]{:S(2)}) copy-start(bf16[128,2048]{1,0:T(8,128)(2,1)} %param.21) | copy-start | bytes 1572868
  6.6 181.2 %all-gather.2.cloned.1.call-start = ((), (), s32[]{:S(2)}) async-start(), calls=%async_computation.3 | async-start | bytes 17039360 | tf_op jit(solution)/shard_map/all_gather | solution.py:20
  15.3 25.4 %copy-start.5 = (f32[1,512]{1,0:T(1,128)S(1)}, f32[1,512]{1,0:T(1,128)}, u32[]{:S(2)}) copy-start(f32[1,512]{1,0:T(1,128)} %param.17) | copy-start | bytes 6148
  15.5 6.3 %collective-permute-start = (bf16[1,144,128]{2,1,0:T(8,128)(2,1)S(1)}, bf16[1,144,128]{2,1,0:T(8,128)(2,1)S(1)}, u32[]{:S(2)}, u32[]{:S(2)}) collective-permute-start(bf16[1,144,128]{2,1,0:T(8,128)(2,1)S(1)} %fusion.41), channel_id=1, source_target_pairs={{0,8},{16,24},{32,40},{48,56},{64,72},{80,88},{96,104},{112,120},{... | collective-permute-start | bytes 110600 | tf_op jit(solution)/shard_map/ppermute | solution.py:57
  22.0 0.7 collective-permute-start.1
  22.7 19.4 %copy-start.2 = (bf16[512,128]{1,0:T(8,128)(2,1)S(1)}, bf16[512,128]{1,0:T(8,128)(2,1)}, u32[]{:S(2)}) copy-start(bf16[512,128]{1,0:T(8,128)(2,1)} %param.13) | copy-start | bytes 393220
  22.9 0.7 collective-permute-start.2
  23.8 18.8 %copy-start.1 = (bf16[512,128]{1,0:T(8,128)(2,1)S(1)}, bf16[512,128]{1,0:T(8,128)(2,1)}, u32[]{:S(2)}) copy-start(bf16[512,128]{1,0:T(8,128)(2,1)} %param.15) | copy-start | bytes 393220
  23.8 0.8 collective-permute-start.3
  24.8 0.7 collective-permute-start.4
  25.7 0.7 collective-permute-start.5
  26.6 0.7 collective-permute-start.6
  27.3 16.2 %copy-start.4 = (bf16[512,128]{1,0:T(8,128)(2,1)S(1)}, bf16[512,128]{1,0:T(8,128)(2,1)}, u32[]{:S(2)}) copy-start(bf16[512,128]{1,0:T(8,128)(2,1)} %param.16) | copy-start | bytes 393220
  27.3 16.2 %copy-start.7 = (f32[128]{0:T(128)S(1)}, f32[128]{0:T(128)}, u32[]{:S(2)}) copy-start(f32[128]{0:T(128)} %param.20) | copy-start | bytes 1540
  27.5 0.8 collective-permute-start.7
  28.5 13.2 %collective-permute-start.8 = (bf16[1,144,128]{2,1,0:T(8,128)(2,1)S(1)}, bf16[1,144,128]{2,1,0:T(8,128)(2,1)S(1)}, u32[]{:S(2)}, u32[]{:S(2)}) collective-permute-start(bf16[1,144,128]{2,1,0:T(8,128)(2,1)S(1)} %fusion.49), channel_id=1, source_target_pairs={{0,8},{8,16},{16,24},{24,32},{32,40},{40,48},{48,56},{56,64},{64,7... | collective-permute-start | bytes 110600 | tf_op jit(solution)/shard_map/ppermute | solution.py:57
  44.5 40.3 %collective-permute-start.9 = (bf16[256,2048]{1,0:T(8,128)(2,1)S(1)}, bf16[256,2048]{1,0:T(8,128)(2,1)S(1)}, u32[]{:S(2)}, u32[]{:S(2)}) collective-permute-start(bf16[256,2048]{1,0:T(8,128)(2,1)S(1)} %slice.203), channel_id=1, source_target_pairs={{0,1},{1,0},{2,3},{3,2},{4,5},{5,4},{6,7},{7,6},{8,9},{9,8},{10,11... | collective-permute-start | bytes 3145736 | tf_op jit(solution)/shard_map/ppermute | solution.py:87
  85.3 17.6 %copy-start.3 = (bf16[64,2048]{1,0:T(8,128)(2,1)S(1)}, bf16[64,2048]{1,0:T(8,128)(2,1)}, u32[]{:S(2)}) copy-start(bf16[64,2048]{1,0:T(8,128)(2,1)} %param.22) | copy-start | bytes 786436
  85.3 17.8 %copy-start.6 = (f32[2048]{0:T(1024)S(1)}, f32[2048]{0:T(1024)}, u32[]{:S(2)}) copy-start(f32[2048]{0:T(1024)} %param.23) | copy-start | bytes 24580
Sparse Core Ops, SparseCore 0:
  9.5 178.2 all-gather.1
